TPU v7x, 32 devices: a whole 2x2x4 slice. The times are simulated.
32 devices in a mesh: sp: 4 (over y, x), tp: 8 (over z, core).
Axes of the slice: x: 2, y: 2, z: 4, core: 2. Of those that a mesh axis runs over, the one named last changes fastest.
Arguments:
- queries: bfloat16 [4096, 1024], P('sp', 'tp'), may hold values from -18 to 18
- keys: bfloat16 [4096, 256], P('sp'), may hold values from -18 to 18
- values: bfloat16 [4096, 256], P('sp'), may hold values from -6 to 6
- sink_logits: float32 [16], P('tp'), may hold values from 3 to 7
- w_out: bfloat16 [1024, 2048], P('tp'), may hold values from -1.5 to 1.5
- residual: bfloat16 [4096, 2048], P(('sp', 'tp')), may hold values from -6 to 6
- norm_gain: float32 [2048], replicated, may hold values from 0.1 to 1.9
- expert_ids: int32 [4096, 4], P('sp'), may hold values from 0 to 15, all different within a row; in each aligned block of 1024 rows (0 to 1023, 1024 to 2047, ...) at most 512 rows name the same one
- expert_weights: float32 [4096, 4], P('sp'), may hold values from 0.1 to 1.5
- w_gate: bfloat16 [32, 768, 2048], P(('sp', 'tp')), may hold values from -0.125 to 0.125
- w_up: bfloat16 [32, 768, 2048], P(('sp', 'tp')), may hold values from -0.125 to 0.125
- w_down: bfloat16 [32, 768, 2048], P(('sp', 'tp')), may hold values from -0.15625 to 0.15625
- shared_gate: bfloat16 [512, 2048], P('tp'), may hold values from -0.125 to 0.125
- shared_up: bfloat16 [512, 2048], P('tp'), may hold values from -0.125 to 0.125
- shared_down: bfloat16 [512, 2048], P('tp'), may hold values from -0.25 to 0.25
Outputs:
- layer_out: bfloat16 [4096, 2048], P(('sp', 'tp'))
Inputs may be any that keep to these rules, and one draw needn't show every extreme that they name: `expert_ids`: each row names 4 different experts; in each aligned block of 1024 rows no expert is named by more than 512 rows.
All inputs are finite; a program needn't handle non-finite values.
Results may differ from a plain program's by a relative error of at most 0.02.
Values may be sent and summed in bfloat16 or wider, within the bound.
A program may use at most 128 MiB of HBM per device.

v0:
```python
import jax
import jax.numpy as jnp
from jax import lax
from jax.sharding import PartitionSpec as P

HD = 64
GROUP = 4
WINDOW = 128
TOPK = 4


def shifted(block, axis, distance):
    devices = range(lax.axis_size(axis))
    route = [(i - distance, i) for i in devices if i - distance in devices]
    return lax.ppermute(block, axis, route)


def from_partner(x, axis, apart):
    return lax.ppermute(x, axis, [(i, i ^ 1 << apart) for i in range(lax.axis_size(axis))])


def normalize(after_mix, norm_gain):
    values_f = after_mix.astype(jnp.float32)
    scale = lax.rsqrt(jnp.mean(values_f * values_f, axis=-1, keepdims=True) + 1e-06)
    return (values_f * scale * norm_gain).astype(jnp.bfloat16)


def slot_layout(route_ids, expert_count, capacity):
    flat_ids = route_ids.reshape(-1)
    matches = (flat_ids[:, None] == jnp.arange(expert_count, dtype=jnp.int32)[None, :]).astype(
        jnp.int32
    )
    earlier = jnp.cumsum(matches, axis=0) - matches
    order_in = jnp.sum(earlier * matches, axis=1)
    slot_index = flat_ids * capacity + order_in
    owners = jnp.arange(flat_ids.shape[0], dtype=jnp.int32) // TOPK
    slot_owner = jnp.full((expert_count * capacity,), -1, jnp.int32).at[slot_index].set(owners)
    return (slot_index, slot_owner)


def body(
    queries,
    keys,
    values,
    sink_logits,
    w_out,
    residual,
    norm_gain,
    expert_ids,
    expert_weights,
    w_gate,
    w_up,
    w_down,
    shared_gate,
    shared_up,
    shared_down,
):
    tp_count = lax.axis_size("tp")
    sp_count = lax.axis_size("sp")
    seq_rows = queries.shape[0]
    expert_count = sp_count * tp_count // 2
    capacity = max(2, 2 * seq_rows * TOPK // expert_count)
    local_heads = queries.shape[1] // HD
    kv_start = lax.axis_index("tp") * local_heads // GROUP * HD
    key_cols = lax.dynamic_slice_in_dim(keys, kv_start, HD, 1)
    value_cols = lax.dynamic_slice_in_dim(values, kv_start, HD, 1)
    rim_keys, rim_values = shifted(
        (key_cols[seq_rows - WINDOW :], value_cols[seq_rows - WINDOW :]), "sp", 1
    )
    num_blocks = seq_rows // WINDOW
    key_blocks = key_cols.reshape(num_blocks, WINDOW, HD)
    value_blocks = value_cols.reshape(num_blocks, WINDOW, HD)
    keys_ext = jnp.concatenate(
        [jnp.concatenate([rim_keys[None], key_blocks[:-1]], axis=0), key_blocks], axis=1
    )
    values_ext = jnp.concatenate(
        [jnp.concatenate([rim_values[None], value_blocks[:-1]], axis=0), value_blocks], axis=1
    )
    query_blocks = queries.reshape(num_blocks, WINDOW, local_heads, HD)
    scores = jnp.einsum(
        "nqhd,nsd->nhqs", query_blocks, keys_ext, preferred_element_type=jnp.float32
    ) * HD ** (-0.5)
    query_pos = jnp.arange(WINDOW)[:, None] + WINDOW
    key_pos = jnp.arange(2 * WINDOW)[None, :]
    in_band = (key_pos <= query_pos) & (key_pos > query_pos - WINDOW)
    absolute = (
        lax.axis_index("sp") * seq_rows
        + jnp.arange(num_blocks)[:, None, None] * WINDOW
        + key_pos[None]
        - WINDOW
    )
    allowed = in_band[None] & (absolute >= 0)
    scores = jnp.where(allowed[:, None], scores, -jnp.inf)
    sink_col = jnp.broadcast_to(sink_logits[None, :, None, None], scores.shape[:-1] + (1,))
    combined = jnp.concatenate([scores, sink_col], axis=-1)
    row_max = jnp.max(combined, axis=-1, keepdims=True)
    exps = jnp.exp(combined - row_max)
    weights = (exps[..., :-1] / jnp.sum(exps, axis=-1, keepdims=True)).astype(jnp.bfloat16)
    attended = jnp.einsum("nhqs,nsd->nqhd", weights, values_ext, preferred_element_type=jnp.float32)
    attended = attended.astype(jnp.bfloat16).reshape(seq_rows, local_heads * HD)
    head_rows = lax.all_to_all(attended, "tp", split_axis=0, concat_axis=1, tiled=True)
    projected = jnp.dot(
        head_rows,
        lax.all_gather(w_out, "tp", axis=0, tiled=True),
        preferred_element_type=jnp.float32,
    )
    after_mix = (residual.astype(jnp.float32) + projected).astype(jnp.bfloat16)
    normed = normalize(after_mix, norm_gain)
    tp_index = lax.axis_index("tp")
    lanes = tp_count // 2
    lane = tp_index // 2
    keep = tp_index % 2
    half_cap = capacity // 2
    slot_index, slot_owner = slot_layout(expert_ids, expert_count, capacity)
    all_rows = lax.all_gather(normed, "tp", axis=0, tiled=True)
    lane_owner = lax.dynamic_slice_in_dim(slot_owner.reshape(sp_count, lanes, capacity), lane, 1, 1)
    lane_owner = lane_owner.reshape(sp_count * capacity)
    picked = all_rows[jnp.maximum(lane_owner, 0)]
    outgoing = jnp.where((lane_owner >= 0)[:, None], picked, jnp.zeros((), jnp.bfloat16))
    arrived = lax.all_to_all(
        outgoing.reshape(sp_count, capacity, -1), "sp", split_axis=0, concat_axis=0, tiled=True
    )
    arrived = arrived.reshape(sp_count * capacity, -1)
    gate_act = jnp.einsum("td,fd->tf", arrived, w_gate[0], preferred_element_type=jnp.float32)
    up_act = jnp.einsum("td,fd->tf", arrived, w_up[0], preferred_element_type=jnp.float32)
    hidden = (jax.nn.silu(gate_act) * up_act).astype(jnp.bfloat16)
    half_out = jnp.dot(hidden, w_down[0], preferred_element_type=jnp.float32).astype(jnp.bfloat16)
    half_out = half_out.reshape(sp_count, 2, half_cap, -1)
    mine = lax.dynamic_index_in_dim(half_out, keep, 1, keepdims=False)
    other = lax.dynamic_index_in_dim(half_out, 1 - keep, 1, keepdims=False)
    partner = from_partner(other, "tp", 0)
    expert_sum = (mine.astype(jnp.float32) + partner.astype(jnp.float32)).astype(jnp.bfloat16)
    held = lax.all_to_all(expert_sum, "sp", split_axis=0, concat_axis=0, tiled=True).reshape(
        sp_count * half_cap, -1
    )
    route_rank = slot_index.reshape(seq_rows, TOPK) - expert_ids * capacity
    held_here = (expert_ids % lanes == lane) & (route_rank // half_cap == keep)
    position = expert_ids // lanes * half_cap + route_rank % half_cap
    scaled = jnp.where(held_here, expert_weights, jnp.zeros((), expert_weights.dtype))
    shared_gate_act = jnp.einsum(
        "td,fd->tf", all_rows, shared_gate, preferred_element_type=jnp.float32
    )
    shared_up_act = jnp.einsum("td,fd->tf", all_rows, shared_up, preferred_element_type=jnp.float32)
    shared_hidden = (jax.nn.silu(shared_gate_act) * shared_up_act).astype(jnp.bfloat16)
    partial_sum = jnp.dot(shared_hidden, shared_down, preferred_element_type=jnp.float32)
    for route_slot in range(TOPK):
        partial_sum = partial_sum + scaled[:, route_slot : route_slot + 1] * held[
            position[:, route_slot]
        ].astype(jnp.float32)
    moe_sum = lax.psum_scatter(
        partial_sum.astype(jnp.bfloat16), "tp", scatter_dimension=0, tiled=True
    )
    return (after_mix.astype(jnp.float32) + moe_sum.astype(jnp.float32)).astype(jnp.bfloat16)


def solution(mesh):
    return jax.shard_map(
        body,
        mesh=mesh,
        in_specs=(
            P("sp", "tp"),
            P("sp", None),
            P("sp", None),
            P("tp"),
            P("tp", None),
            P(("sp", "tp"), None),
            P(),
            P("sp", None),
            P("sp", None),
            P(("sp", "tp"), None, None),
            P(("sp", "tp"), None, None),
            P(("sp", "tp"), None, None),
            P("tp", None),
            P("tp", None),
            P("tp", None),
        ),
        out_specs=P(("sp", "tp"), None),
        check_vma=False,
    )
```

profile of v0, /device:TPU:0, one launch (start us, length us, event | category | flops | bytes accessed | tf_op | source)
XLA Modules:
  0.0 462.0 jit_solution(13587522794302528692)
XLA Ops:
  7.3 2.1 constant_dynamic-slice_fusion
  10.1 5.5 %collective-permute-start.1 = (bf16[128,64]{0,1:T(8,128)(2,1)}, bf16[128,64]{0,1:T(8,128)(2,1)}, u32[]{:S(2)}, u32[]{:S(2)}) collective-permute-start(bf16[128,64]{0,1:T(8,128)(2,1)} %slice.80), channel_id=1, source_target_pairs={{0,8},{8,16},{16,24},{1,9},{9,17},{17,25},{2,10},{10,18},{18,26},{... | collective-permute-start | bytes 49160 | tf_op jit(solution)/shard_map/ppermute | solution.py:15
  16.7 3.4 collective-permute-start
  22.7 2.0 reshape.266
  24.7 1.8 fusion.58
  28.0 21.9 %all_to_all.29 = bf16[8,128,128]{1,2,0:T(8,128)(2,1)S(1)} all-to-all(bf16[8,128,128]{1,2,0:T(8,128)(2,1)S(1)} %bitcast.99), channel_id=1, replica_groups=mesh['sp'=4,'tp'=8] {'tp'}, dimensions={0} | all-to-all | bytes 524288 | tf_op jit(solution)/shard_map/all_to_all | solution.py:101
  50.0 14.2 %all-gather.3.cloned.1.call-done = bf16[1024,2048]{1,0:T(8,128)(2,1)} async-done(((bf16[128,2048]{1,0:T(8,128)(2,1)}), bf16[1024,2048]{1,0:T(8,128)(2,1)}) %all-gather.3.cloned.1.call-update) | async-done | bytes 4194320 | tf_op jit(solution)/shard_map/all_gather | solution.py:104
  64.2 3.1 multiply_reduce_fusion
  73.8 8.3 %reduce-window.6 = s32[16,32,128]{2,1,0:T(8,128)S(1)} reduce-window(s32[16,32,128]{2,1,0:T(8,128)} %fusion.45, s32[]{:T(128)} %constant.127.clone.1), window={size=1x1x128 pad=0_0x0_0x127_0}, to_apply=%region_3.4 | reduce-window | flops 8323072 | bytes 524292 | tf_op jit(solution)/shard_map/reduce-window
  83.8 1.4 mul.144
  85.6 15.5 %scatter_custom_fusion = s32[8192]{0:T(1024)S(1)} fusion(s32[4096]{0:T(1024)S(1)} %bitcast.103, s32[4096]{0:T(1024)S(1)} %add_select_fusion.4, s32[]{:T(128)} %constant.132.clone.1), kind=kCustom, calls=%fused_computation.110 | custom fusion | bytes 32772 | tf_op jit(solution)/shard_map/scatter | solution.py:37
  101.2 13.8 %all-gather.5.cloned.1.call-done = bf16[1024,2048]{1,0:T(8,128)(2,1)} async-done(((bf16[128,2048]{1,0:T(8,128)(2,1)}), bf16[1024,2048]{1,0:T(8,128)(2,1)}) %all-gather.5.cloned.1.call-update) | async-done | bytes 4194320 | tf_op jit(solution)/shard_map/all_gather | solution.py:115
  115.0 19.0 %gather_fusion = bf16[2048,2048]{1,0:T(8,128)(2,1)} fusion(bf16[1024,2048]{1,0:T(8,128)(2,1)} %all-gather.5.cloned.1.call-done, s32[2048]{0:T(1024)S(1)} %broadcast_clamp_fusion), kind=kCustom, calls=%fused_computation | custom fusion | bytes 16785408 | tf_op jit(solution)/shard_map/gather | solution.py:118
  134.1 7.3 %broadcast_select_fusion = bf16[4,512,2048]{2,1,0:T(8,128)(2,1)} fusion(bf16[4,512,2048]{2,1,0:T(8,128)(2,1)} %bitcast.94, pred[4,512]{1,0:T(4,128)(4,1)S(1)} %bitcast.104), kind=kLoop, calls=%fused_computation.9 | loop fusion | flops 4194304 | bytes 16779264 | tf_op jit(solution)/shard_map/jit(_where)/select_n | solution.py:119
  141.3 5.9 %all-to-all-start.1 = ((bf16[4,512,2048]{2,1,0:T(8,128)(2,1)}), bf16[4,512,2048]{2,1,0:T(8,128)(2,1)}, u32[]{:S(2)}, u32[]{:S(2)}) async-start(bf16[4,512,2048]{2,1,0:T(8,128)(2,1)} %broadcast_select_fusion), calls=%async_computation.1 | async-start | bytes 16777216 | tf_op jit(solution)/shard_map/all_to_all | solution.py:120
  147.2 92.8 %all-to-all-done.1 = bf16[4,512,2048]{2,1,0:T(8,128)(2,1)} async-done(((bf16[4,512,2048]{2,1,0:T(8,128)(2,1)}), bf16[4,512,2048]{2,1,0:T(8,128)(2,1)}, u32[]{:S(2)}, u32[]{:S(2)}) %all-to-all-start.1) | async-done | bytes 8388640 | tf_op jit(solution)/shard_map/all_to_all | solution.py:120
  240.1 11.8 %fusion.4 = f32[2048,768]{1,0:T(8,128)} fusion(bf16[2048,2048]{1,0:T(8,128)(2,1)} %bitcast.16, bf16[1,768,2048]{2,1,0:T(8,128)(2,1)} %param.24), kind=kOutput, calls=%fused_computation.15 | convolution fusion | flops 6442450944 | bytes 17825792 | tf_op jit(solution)/shard_map/td,fd->tf/dot_general | solution.py:124
  251.8 21.3 %convolution_convert_fusion = bf16[2048,2048]{1,0:T(8,128)(2,1)} fusion(f32[2048,768]{1,0:T(8,128)} %fusion.4, bf16[2048,2048]{1,0:T(8,128)(2,1)} %bitcast.16, bf16[1,768,2048]{2,1,0:T(8,128)(2,1)S(1)} %copy-done, bf16[1,768,2048]{2,1,0:T(8,128)(2,1)} %param.25), kind=kOutput, calls=%fused_computation.10 | convolution fusion | flops 12898533376 | bytes 29360128 | tf_op jit(solution)/shard_map/dot_general | solution.py:127
  273.2 4.7 %dynamic-slice_bitcast_fusion = bf16[4,256,2048]{2,1,0:T(8,128)(2,1)} fusion(bf16[4,2,256,2048]{3,2,1,0:T(8,128)(2,1)} %bitcast.95, s32[]{:T(128)S(6)} %select_n.104), kind=kLoop, calls=%fused_computation.12 | loop fusion | bytes 8388612 | tf_op jit(solution)/shard_map/jit(dynamic_index_in_dim)/squeeze | solution.py:130
  277.9 7.5 %collective-permute-done.2 = bf16[4,256,2048]{2,1,0:T(8,128)(2,1)} collective-permute-done((bf16[4,256,2048]{2,1,0:T(8,128)(2,1)}, bf16[4,256,2048]{2,1,0:T(8,128)(2,1)}, u32[]{:S(2)}, u32[]{:S(2)}) %collective-permute-start.2) | collective-permute-done | bytes 4194336 | tf_op jit(solution)/shard_map/ppermute | solution.py:19
  285.4 7.7 %fusion = bf16[4,256,2048]{2,1,0:T(8,128)(2,1)} fusion(bf16[4,256,2048]{2,1,0:T(8,128)(2,1)} %collective-permute-done.2, bf16[4,2,256,2048]{3,2,1,0:T(8,128)(2,1)} %bitcast.96, s32[]{:T(128)S(6)} %select_n.103), kind=kLoop, calls=%fused_computation.7 | loop fusion | flops 8388608 | bytes 12582916 | tf_op jit(solution)/shard_map/convert_element_type | solution.py:132
  293.1 5.1 %all-to-all-start.2 = ((bf16[4,256,2048]{2,1,0:T(8,128)(2,1)}), bf16[4,256,2048]{2,1,0:T(8,128)(2,1)}, u32[]{:S(2)}, u32[]{:S(2)}) async-start(bf16[4,256,2048]{2,1,0:T(8,128)(2,1)} %fusion), calls=%async_computation.2 | async-start | bytes 8388608 | tf_op jit(solution)/shard_map/all_to_all | solution.py:133
  302.9 1.4 fusion.59
  304.3 8.0 %fusion.12 = f32[1024,2048]{1,0:T(8,128)} fusion(bf16[64,2048]{1,0:T(8,128)(2,1)S(1)} %copy-done.6, bf16[1024,2048]{1,0:T(8,128)(2,1)} %all-gather.5.cloned.1.call-done, bf16[64,2048]{1,0:T(8,128)(2,1)S(1)} %copy-done.7, f32[1024,64]{0,1:T(8,128)S(1)} %fusion.59), kind=kOutput, calls=%fused_computation.33 | convolution fusion | flops 537264128 | bytes 13369344 | tf_op jit(solution)/shard_map/dot_general | solution.py:145
  312.3 33.9 %all-to-all-done.2 = bf16[4,256,2048]{2,1,0:T(8,128)(2,1)} async-done(((bf16[4,256,2048]{2,1,0:T(8,128)(2,1)}), bf16[4,256,2048]{2,1,0:T(8,128)(2,1)}, u32[]{:S(2)}, u32[]{:S(2)}) %all-to-all-start.2) | async-done | bytes 4194336 | tf_op jit(solution)/shard_map/all_to_all | solution.py:133
  346.2 11.8 %gather_fusion.1 = bf16[1024,2048]{1,0:T(8,128)(2,1)} fusion(bf16[1024,2048]{1,0:T(8,128)(2,1)} %bitcast.23, s32[1024]{0:T(1024)S(1)} %get-tuple-element.24), kind=kCustom, calls=%fused_computation.1 | custom fusion | bytes 8392704 | tf_op jit(solution)/shard_map/gather | solution.py:147
  358.0 11.6 %gather_fusion.2 = bf16[1024,2048]{1,0:T(8,128)(2,1)} fusion(bf16[1024,2048]{1,0:T(8,128)(2,1)} %bitcast.23, s32[1024]{0:T(1024)S(1)} %get-tuple-element.23), kind=kCustom, calls=%fused_computation.2 | custom fusion | bytes 8392704 | tf_op jit(solution)/shard_map/gather | solution.py:147
  369.6 11.5 %gather_fusion.3 = bf16[1024,2048]{1,0:T(8,128)(2,1)} fusion(bf16[1024,2048]{1,0:T(8,128)(2,1)} %bitcast.23, s32[1024]{0:T(1024)S(1)} %get-tuple-element.22), kind=kCustom, calls=%fused_computation.3 | custom fusion | bytes 8392704 | tf_op jit(solution)/shard_map/gather | solution.py:147
  381.1 11.6 %gather_fusion.4 = bf16[1024,2048]{1,0:T(8,128)(2,1)} fusion(bf16[1024,2048]{1,0:T(8,128)(2,1)} %bitcast.23, s32[1024]{0:T(1024)S(1)} %get-tuple-element.21), kind=kCustom, calls=%fused_computation.4 | custom fusion | bytes 8392704 | tf_op jit(solution)/shard_map/gather | solution.py:147
  392.7 12.4 %add_convert_fusion = bf16[1024,2048]{1,0:T(8,128)(2,1)} fusion(bf16[1024,2048]{1,0:T(8,128)(2,1)} %gather_fusion.4, bf16[1024,2048]{1,0:T(8,128)(2,1)} %gather_fusion.3, bf16[1024,2048]{1,0:T(8,128)(2,1)} %gather_fusion.2, f32[1024,2048]{1,0:T(8,128)} %fusion.12, bf16[1024,2048]{1,0:T(8,128)(2,1)} %gather_fusion.1, f32[1024]{0:T(1024)S(1)} %get-tuple-element.6, ...), kind=kLoop, calls=%fused_computation.8 | loop fusion | flops 27262976 | bytes 29376512 | tf_op jit(solution)/shard_map/convert_element_type | solution.py:151
  405.1 48.2 %reduce-scatter.2.cloned.1.call-done = bf16[128,2048]{1,0:T(8,128)(2,1)} async-done(((bf16[1024,2048]{1,0:T(8,128)(2,1)}), bf16[128,2048]{1,0:T(8,128)(2,1)}) %reduce-scatter.2.cloned.1.call-update) | async-done | bytes 524304 | tf_op jit(solution)/shard_map/reduce_scatter | solution.py:150
  453.2 2.3 add_convert_fusion.1
  (81 shorter events, 19.7 us)
Async XLA Ops:
  6.5 245.3 %copy-start = (bf16[1,768,2048]{2,1,0:T(8,128)(2,1)S(1)}, bf16[1,768,2048]{2,1,0:T(8,128)(2,1)}, u32[]{:S(2)}) copy-start(bf16[1,768,2048]{2,1,0:T(8,128)(2,1)} %param.26) | copy-start | bytes 9437188
  6.5 57.6 %all-gather.3.cloned.1.call-start = ((), (), s32[]{:S(2)}) async-start(), calls=%async_computation.4 | async-start | bytes 4718592 | tf_op jit(solution)/shard_map/all_gather | solution.py:104
  7.3 107.8 %all-gather.5.cloned.1.call-start = ((), (), s32[]{:S(2)}) async-start(), calls=%async_computation.5 | async-start | bytes 4718592 | tf_op jit(solution)/shard_map/all_gather | solution.py:115
  10.1 14.5 %collective-permute-start.1 = (bf16[128,64]{0,1:T(8,128)(2,1)}, bf16[128,64]{0,1:T(8,128)(2,1)}, u32[]{:S(2)}, u32[]{:S(2)}) collective-permute-start(bf16[128,64]{0,1:T(8,128)(2,1)} %slice.80), channel_id=1, source_target_pairs={{0,8},{8,16},{16,24},{1,9},{9,17},{17,25},{2,10},{10,18},{18,26},{... | collective-permute-start | bytes 49160 | tf_op jit(solution)/shard_map/ppermute | solution.py:15
  16.7 10.3 %collective-permute-start = (bf16[128,64]{0,1:T(8,128)(2,1)S(1)}, bf16[128,64]{0,1:T(8,128)(2,1)}, u32[]{:S(2)}, u32[]{:S(2)}) collective-permute-start(bf16[128,64]{0,1:T(8,128)(2,1)S(1)} %slice.78), channel_id=1, source_target_pairs={{0,8},{8,16},{16,24},{1,9},{9,17},{17,25},{2,10},{10,18},{18,26},{... | collective-permute-start | bytes 49160 | tf_op jit(solution)/shard_map/ppermute | solution.py:15
  22.7 3.8 copy-start.12
  24.7 2.3 copy-start.9
  28.0 40.3 %copy-start.11 = (f32[2048]{0:T(1024)S(1)}, f32[2048]{0:T(1024)}, u32[]{:S(2)}) copy-start(f32[2048]{0:T(1024)} %param.21) | copy-start | bytes 24580
  50.0 19.4 %copy-start.8 = (s32[1024,4]{0,1:T(4,128)S(1)}, s32[1024,4]{0,1:T(4,128)}, u32[]{:S(2)}) copy-start(s32[1024,4]{0,1:T(4,128)} %param.22) | copy-start | bytes 49156
  67.3 1.1 copy-start.4
  141.3 98.7 %all-to-all-start.1 = ((bf16[4,512,2048]{2,1,0:T(8,128)(2,1)}), bf16[4,512,2048]{2,1,0:T(8,128)(2,1)}, u32[]{:S(2)}, u32[]{:S(2)}) async-start(bf16[4,512,2048]{2,1,0:T(8,128)(2,1)} %broadcast_select_fusion), calls=%async_computation.1 | async-start | bytes 16777216 | tf_op jit(solution)/shard_map/all_to_all | solution.py:120
  277.9 7.5 %collective-permute-start.2 = (bf16[4,256,2048]{2,1,0:T(8,128)(2,1)}, bf16[4,256,2048]{2,1,0:T(8,128)(2,1)}, u32[]{:S(2)}, u32[]{:S(2)}) collective-permute-start(bf16[4,256,2048]{2,1,0:T(8,128)(2,1)} %dynamic-slice_bitcast_fusion), channel_id=1, source_target_pairs={{0,1},{1,0},{2,3},{3,2},{4,5},{5,4},{6,7},{7,6},{8,9},{9,8},{10,11... | collective-permute-start | bytes 12582920 | tf_op jit(solution)/shard_map/ppermute | solution.py:19
  293.1 6.2 %copy-start.10 = (f32[1024,4]{0,1:T(4,128)S(1)}, f32[1024,4]{0,1:T(4,128)}, u32[]{:S(2)}) copy-start(f32[1024,4]{0,1:T(4,128)} %param.23) | copy-start | bytes 49156
  293.1 6.4 %copy-start.3 = (s32[1024,4]{1,0:T(8,128)S(1)}, s32[1024,4]{1,0:T(8,128)}, u32[]{:S(2)}) copy-start(s32[1024,4]{1,0:T(8,128)} %copy.50) | copy-start | bytes 49156
  293.1 53.1 %all-to-all-start.2 = ((bf16[4,256,2048]{2,1,0:T(8,128)(2,1)}), bf16[4,256,2048]{2,1,0:T(8,128)(2,1)}, u32[]{:S(2)}, u32[]{:S(2)}) async-start(bf16[4,256,2048]{2,1,0:T(8,128)(2,1)} %fusion), calls=%async_computation.2 | async-start | bytes 8388608 | tf_op jit(solution)/shard_map/all_to_all | solution.py:133
  298.2 155.0 %reduce-scatter.2.cloned.1.call-start = ((), (), s32[]{:S(2)}) async-start(), calls=%async_computation.6 | async-start | bytes 4718592 | tf_op jit(solution)/shard_map/reduce_scatter | solution.py:150
  299.6 3.3 copy-start.2
  299.6 3.3 copy-start.5
  301.8 2.5 copy-start.6
  301.8 2.5 copy-start.7
  392.7 62.8 %copy-start.1 = (bf16[1,768,2048]{2,1,0:T(8,128)(2,1)S(1)}, bf16[1,768,2048]{2,1,0:T(8,128)(2,1)}, u32[]{:S(2)}) copy-start(bf16[1,768,2048]{2,1,0:T(8,128)(2,1)} %param.26) | copy-start | bytes 9437188
Sparse Core Ops, SparseCore 0:
  8.9 55.1 all-gather.2
  69.5 45.5 all-gather.4
  405.2 47.9 reduce-scatter.1
where the time goes:
time: 464 us; the launch traced here: 462 us
  waiting for transfers between devices  211 us (45%)
  local copies, waits for them, and re-layouts  103 us (22%)
  matrix products  48.4 us (10%)
  other arithmetic  43.9 us (9%)
  blocking collectives  21.9 us (5%)
  starting transfers between devices  20.1 us (4%)
  between operations  13.5 us (3%)
    all_to_all x1, waiting for transfers between devices, body(): lax.all_to_all(outgoing.reshape(sp_count, capacity, -1), 'sp', split_axis...  92.8 us
    reduce_scatter x1, waiting for transfers between devices, body(): lax.psum_scatter(partial_sum.astype(jnp.bfloat16), 'tp', scatter_dimensio...  48.2 us
    gather x4, local copies, waits for them, and re-layouts, body(): held[position[:, route_slot]].astype(jnp.float32)  46.5 us
    all_to_all x1, waiting for transfers between devices, body(): lax.all_to_all(expert_sum, 'sp', split_axis=0, concat_axis=0, tiled=True)  33.9 us
    all_to_all x1, blocking collectives, body(): lax.all_to_all(attended, 'tp', split_axis=0, concat_axis=1, tiled=True)  21.9 us
    dot_general x1, matrix products, body(): jnp.dot(hidden, w_down[0], preferred_element_type=jnp.float32)  21.3 us
    gather x1, local copies, waits for them, and re-layouts, body(): picked = all_rows[jnp.maximum(lane_owner, 0)]  19 us
    scatter x1, local copies, waits for them, and re-layouts, slot_layout(): jnp.full((expert_count * capacity,), -1, jnp.int32).at[slot_index]  15.5 us
  transfers between devices with their start and end apart: 8, of which 6 were waited for; matrix products, arithmetic and copies ran while one was open for 12% of the time, Pallas kernels for 0%

commit v1 on v0

v1 whole, which is shorter than its diff:
```python
import jax
import jax.numpy as jnp
from jax import lax
from jax.sharding import PartitionSpec as P

HD = 64
GROUP = 4
WINDOW = 128
TOPK = 4
CHUNKS = 2


def shifted(block, axis, distance):
    devices = range(lax.axis_size(axis))
    route = [(i - distance, i) for i in devices if i - distance in devices]
    return lax.ppermute(block, axis, route)


def from_partner(x, axis, apart):
    return lax.ppermute(x, axis, [(i, i ^ 1 << apart) for i in range(lax.axis_size(axis))])


def normalize(after_mix, norm_gain):
    values_f = after_mix.astype(jnp.float32)
    scale = lax.rsqrt(jnp.mean(values_f * values_f, axis=-1, keepdims=True) + 1e-06)
    return (values_f * scale * norm_gain).astype(jnp.bfloat16)


def lane_slots(route_ids, route_weights, targets, first_rank, half_cap):
    named = route_ids[:, :, None] == targets[None, None, :]
    named_f = jnp.sum(named.astype(jnp.float32), axis=1)
    weight = jnp.sum(jnp.where(named, route_weights[:, :, None], 0.0), axis=1)
    rows = route_ids.shape[0]
    before = jnp.arange(rows)[:, None] > jnp.arange(rows)[None, :]
    rank = jnp.dot(
        before.astype(jnp.bfloat16),
        named_f.astype(jnp.bfloat16),
        preferred_element_type=jnp.float32,
    )
    place = jnp.where(named_f > 0, rank - first_rank, -1.0)
    slots = jnp.arange(half_cap, dtype=jnp.float32)
    picks, mixes = [], []
    for s in range(targets.shape[0]):
        hit = place[:, s : s + 1] == slots[None, :]
        picks.append(jnp.where(hit, 1.0, 0.0).astype(jnp.bfloat16))
        mixes.append(jnp.where(hit, weight[:, s : s + 1], 0.0).astype(jnp.bfloat16))
    return jnp.concatenate(picks, axis=1), jnp.concatenate(mixes, axis=1)


def body(
    queries,
    keys,
    values,
    sink_logits,
    w_out,
    residual,
    norm_gain,
    expert_ids,
    expert_weights,
    w_gate,
    w_up,
    w_down,
    shared_gate,
    shared_up,
    shared_down,
):
    other_gate, other_up, other_down = (from_partner(w[0], "tp", 0) for w in (w_gate, w_up, w_down))
    tp_count = lax.axis_size("tp")
    sp_count = lax.axis_size("sp")
    seq_rows = queries.shape[0]
    expert_count = sp_count * tp_count // 2
    capacity = max(2, 2 * seq_rows * TOPK // expert_count)
    local_heads = queries.shape[1] // HD
    kv_start = lax.axis_index("tp") * local_heads // GROUP * HD
    key_cols = lax.dynamic_slice_in_dim(keys, kv_start, HD, 1)
    value_cols = lax.dynamic_slice_in_dim(values, kv_start, HD, 1)
    rim = jnp.concatenate([keys[seq_rows - WINDOW :], values[seq_rows - WINDOW :]], axis=1)
    rim = shifted(rim, "sp", 1)
    rim_keys = lax.dynamic_slice_in_dim(rim, kv_start, HD, 1)
    rim_values = lax.dynamic_slice_in_dim(rim, kv_start + keys.shape[1], HD, 1)
    num_blocks = seq_rows // WINDOW
    key_blocks = key_cols.reshape(num_blocks, WINDOW, HD)
    value_blocks = value_cols.reshape(num_blocks, WINDOW, HD)
    keys_ext = jnp.concatenate(
        [jnp.concatenate([rim_keys[None], key_blocks[:-1]], axis=0), key_blocks], axis=1
    )
    values_ext = jnp.concatenate(
        [jnp.concatenate([rim_values[None], value_blocks[:-1]], axis=0), value_blocks], axis=1
    )
    query_blocks = queries.reshape(num_blocks, WINDOW, local_heads, HD)
    scores = jnp.einsum(
        "nqhd,nsd->nhqs", query_blocks, keys_ext, preferred_element_type=jnp.float32
    ) * HD ** (-0.5)
    query_pos = jnp.arange(WINDOW)[:, None] + WINDOW
    key_pos = jnp.arange(2 * WINDOW)[None, :]
    in_band = (key_pos <= query_pos) & (key_pos > query_pos - WINDOW)
    absolute = (
        lax.axis_index("sp") * seq_rows
        + jnp.arange(num_blocks)[:, None, None] * WINDOW
        + key_pos[None]
        - WINDOW
    )
    allowed = in_band[None] & (absolute >= 0)
    scores = jnp.where(allowed[:, None], scores, -jnp.inf)
    sink_col = jnp.broadcast_to(sink_logits[None, :, None, None], scores.shape[:-1] + (1,))
    combined = jnp.concatenate([scores, sink_col], axis=-1)
    row_max = jnp.max(combined, axis=-1, keepdims=True)
    exps = jnp.exp(combined - row_max)
    weights = (exps[..., :-1] / jnp.sum(exps, axis=-1, keepdims=True)).astype(jnp.bfloat16)
    attended = jnp.einsum("nhqs,nsd->nqhd", weights, values_ext, preferred_element_type=jnp.float32)
    attended = attended.astype(jnp.bfloat16).reshape(seq_rows, local_heads * HD)
    head_rows = lax.all_to_all(attended, "tp", split_axis=0, concat_axis=1, tiled=True)
    projected = jnp.dot(
        head_rows,
        lax.all_gather(w_out, "tp", axis=0, tiled=True),
        preferred_element_type=jnp.float32,
    )
    after_mix = (residual.astype(jnp.float32) + projected).astype(jnp.bfloat16)
    normed = normalize(after_mix, norm_gain)
    tp_index = lax.axis_index("tp")
    lanes = tp_count // 2
    lane = tp_index // 2
    keep = tp_index % 2
    half_cap = capacity // 2
    targets = jnp.arange(sp_count, dtype=jnp.int32) * lanes + lane
    first_rank = (keep * half_cap).astype(jnp.float32)
    pick, mix = lane_slots(expert_ids, expert_weights, targets, first_rank, half_cap)
    width = after_mix.shape[1]
    step = width // CHUNKS
    gates = [(w_gate[0], w_up[0]), (other_gate, other_up)]
    downs = [w_down[0], other_down]
    sums = [[0.0, 0.0] for _ in gates]
    shared = [0.0, 0.0]
    for c in range(CHUNKS):
        cols = slice(c * step, (c + 1) * step)
        rows = lax.all_gather(normed[:, cols], "tp", axis=0, tiled=True)
        outgoing = lax.dot_general(
            pick, rows, (((0,), (0,)), ((), ())), preferred_element_type=jnp.bfloat16
        )
        arrived = lax.all_to_all(
            outgoing.reshape(sp_count, half_cap, step), "sp", split_axis=0, concat_axis=0, tiled=True
        ).reshape(sp_count * half_cap, step)
        for total, pair in zip(sums, gates):
            for n, w in enumerate(pair):
                total[n] = total[n] + jnp.einsum(
                    "td,fd->tf", arrived, w[:, cols], preferred_element_type=jnp.float32
                )
        for n, w in enumerate((shared_gate, shared_up)):
            shared[n] = shared[n] + jnp.einsum(
                "td,fd->tf", rows, w[:, cols], preferred_element_type=jnp.float32
            )
    shared_hidden = (jax.nn.silu(shared[0]) * shared[1]).astype(jnp.bfloat16)
    hidden = [(jax.nn.silu(g) * u).astype(jnp.bfloat16) for g, u in sums]
    pieces = []
    for c in range(CHUNKS):
        cols = slice(c * step, (c + 1) * step)
        expert_out = sum(
            jnp.dot(h, w[:, cols], preferred_element_type=jnp.float32) for h, w in zip(hidden, downs)
        ).astype(jnp.bfloat16)
        held = lax.all_to_all(
            expert_out.reshape(sp_count, half_cap, step),
            "sp",
            split_axis=0,
            concat_axis=0,
            tiled=True,
        ).reshape(sp_count * half_cap, step)
        part = jnp.dot(shared_hidden, shared_down[:, cols], preferred_element_type=jnp.float32)
        part = part + jnp.dot(mix, held, preferred_element_type=jnp.float32)
        pieces.append(
            lax.psum_scatter(part.astype(jnp.bfloat16), "tp", scatter_dimension=0, tiled=True)
        )
    moe_sum = jnp.concatenate(pieces, axis=1)
    return (after_mix.astype(jnp.float32) + moe_sum.astype(jnp.float32)).astype(jnp.bfloat16)


def solution(mesh):
    return jax.shard_map(
        body,
        mesh=mesh,
        in_specs=(
            P("sp", "tp"),
            P("sp", None),
            P("sp", None),
            P("tp"),
            P("tp", None),
            P(("sp", "tp"), None),
            P(),
            P("sp", None),
            P("sp", None),
            P(("sp", "tp"), None, None),
            P(("sp", "tp"), None, None),
            P(("sp", "tp"), None, None),
            P("tp", None),
            P("tp", None),
            P("tp", None),
        ),
        out_specs=P(("sp", "tp"), None),
        check_vma=False,
    )
```

time: 464 us -> 311 us (0.67)
  local copies, waits for them, and re-layouts: 103 us -> 6.23 us
  waiting for transfers between devices: 211 us -> 140 us
  other arithmetic: 43.9 us -> 6.99 us
  blocking collectives: 21.9 us -> 49.7 us
  matrix products: 48.4 us -> 74.6 us
    all_to_all x2 -> x3, waiting for transfers between devices: 127 us -> 34.3 us  [the longest x1 18.3 us: body(): lax.all_to_all(expert_out.reshape(sp_count, half_cap, step), 'sp', split_...]
    gather x5 -> x0, local copies, waits for them, and re-layouts: 65.5 us -> none  [the longest x4 46.5 us: body(): held[position[:, route_slot]].astype(jnp.float32)]
    all_gather x1 -> x2, waiting for transfers between devices: 13.8 us -> 47.1 us  [body(): rows = lax.all_gather(normed[:, cols], 'tp', axis=0, tiled=True)]
    dot_general x4 -> x23, matrix products: 42.5 us -> 70.7 us  [the longest x8 31.6 us: body(): jnp.einsum('td,fd->tf', arrived, w[:, cols], preferred_element_type=jnp.f...]
    all_to_all x0 -> x1, blocking collectives: none -> 27.3 us  [body(): lax.all_to_all(expert_out.reshape(sp_count, half_cap, step), 'sp', split_...]
    convert_element_type x3 -> x4, other arithmetic: 20.8 us -> 3.91 us  [the longest x2 3.23 us: lane_slots(): mixes.append(jnp.where(hit, weight[:, s:s + 1], 0.0).astype(jnp.bfloat16))]
    scatter x1 -> x0, local copies, waits for them, and re-layouts: 15.5 us -> none  [slot_layout(): jnp.full((expert_count * capacity,), -1, jnp.int32).at[slot_index]]
    reduce_scatter x1 -> x2, waiting for transfers between devices: 48.2 us -> 34.2 us  [body(): lax.psum_scatter(part.astype(jnp.bfloat16), 'tp', scatter_dimension=0, ti...]
  transfers between devices with their start and end apart: 8 -> 12, of which waited for: 6 -> 6; matrix products, arithmetic and copies ran while one was open for 12% -> 22% of each run, Pallas kernels for 0% -> 0%
where the time goes in v1:
time: 311 us; the launch traced here: 310 us
  waiting for transfers between devices  140 us (45%)
  matrix products  74.6 us (24%)
  blocking collectives  49.7 us (16%)
  starting transfers between devices  18.7 us (6%)
  between operations  13.8 us (4%)
  other arithmetic  6.99 us (2%)
  local copies, waits for them, and re-layouts  6.23 us (2%)
    all_gather x2, waiting for transfers between devices, body(): rows = lax.all_gather(normed[:, cols], 'tp', axis=0, tiled=True)  47.1 us
    reduce_scatter x2, waiting for transfers between devices, body(): lax.psum_scatter(part.astype(jnp.bfloat16), 'tp', scatter_dimension=0, ti...  34.2 us
    dot_general x8, matrix products, body(): jnp.einsum('td,fd->tf', arrived, w[:, cols], preferred_element_type=jnp.f...  31.6 us
    all_to_all x1, blocking collectives, body(): lax.all_to_all(expert_out.reshape(sp_count, half_cap, step), 'sp', split_...  27.3 us
    all_gather x1, waiting for transfers between devices, body(): lax.all_gather(w_out, 'tp', axis=0, tiled=True)  23.3 us
    all_to_all x1, blocking collectives, body(): lax.all_to_all(attended, 'tp', split_axis=0, concat_axis=1, tiled=True)  22.4 us
    all_to_all x1, waiting for transfers between devices, body(): lax.all_to_all(expert_out.reshape(sp_count, half_cap, step), 'sp', split_...  18.3 us
    all_to_all x2, waiting for transfers between devices, body(): lax.all_to_all(outgoing.reshape(sp_count, half_cap, step), 'sp', split_ax...  16 us
  transfers between devices with their start and end apart: 12, of which 6 were waited for; matrix products, arithmetic and copies ran while one was open for 22% of the time, Pallas kernels for 0%

profile of v1, /device:TPU:0, one launch (start us, length us, event | category | flops | bytes accessed | tf_op | source)
XLA Modules:
  0.0 310.3 jit_solution(17273013951342688500)
XLA Ops:
  9.1 4.9 %collective-permute-start = (bf16[128,512]{1,0:T(8,128)(2,1)S(1)}, bf16[128,512]{1,0:T(8,128)(2,1)S(1)}, u32[]{:S(2)}, u32[]{:S(2)}) collective-permute-start(bf16[128,512]{1,0:T(8,128)(2,1)S(1)} %pad_maximum_fusion.6), channel_id=1, source_target_pairs={{0,8},{8,16},{16,24},{1,9},{9,17},{17,25},{2,10},{10,18},{18,26},{... | collective-permute-start | bytes 393224 | tf_op jit(solution)/shard_map/ppermute | solution.py:16
  18.5 22.4 %all_to_all.39 = bf16[8,128,128]{1,2,0:T(8,128)(2,1)S(1)} all-to-all(bf16[8,128,128]{1,2,0:T(8,128)(2,1)S(1)} %bitcast.82), channel_id=1, replica_groups=mesh['sp'=4,'tp'=8] {'tp'}, dimensions={0} | all-to-all | bytes 524288 | tf_op jit(solution)/shard_map/all_to_all | solution.py:112
  40.9 23.3 %all-gather.4.cloned.1.call-done = bf16[1024,2048]{1,0:T(8,128)(2,1)} async-done(((bf16[128,2048]{1,0:T(8,128)(2,1)}), bf16[1024,2048]{1,0:T(8,128)(2,1)}) %all-gather.4.cloned.1.call-update) | async-done | bytes 4194320 | tf_op jit(solution)/shard_map/all_gather | solution.py:115
  64.2 3.0 multiply_reduce_fusion
  70.4 25.9 %all-gather.6.cloned.1.call-done = bf16[1024,1024]{1,0:T(8,128)(2,1)} async-done(((bf16[128,1024]{1,0:T(8,128)(2,1)}), bf16[1024,1024]{1,0:T(8,128)(2,1)}) %all-gather.6.cloned.1.call-update) | async-done | bytes 2097168 | tf_op jit(solution)/shard_map/all_gather | solution.py:136
  96.3 5.3 %fusion.34 = bf16[1024,1024]{1,0:T(8,128)(2,1)} fusion(bf16[1024,1024]{1,0:T(8,128)(2,1)} %all-gather.6.cloned.1.call-done, bf16[1024,256]{1,0:T(8,128)(2,1)S(1)} %get-tuple-element.29, bf16[1024,256]{1,0:T(8,128)(2,1)S(1)} %get-tuple-element.30, bf16[1024,256]{1,0:T(8,128)(2,1)S(1)} %get-tuple-element.31, bf16[1024,256]{1,0:T(8,128)(2,1)S(1)} %get-tuple-element.32), kind=kOutput, calls=%fused_computation.65 | convolution fusion | flops 2155872256 | bytes 6291456 | tf_op jit(solution)/shard_map/dot_general | solution.py:137
  101.6 3.7 %all-to-all-start.1 = ((bf16[4,256,1024]{2,1,0:T(8,128)(2,1)}), bf16[4,256,1024]{2,1,0:T(8,128)(2,1)S(1)}, u32[]{:S(2)}, u32[]{:S(2)}) async-start(bf16[4,256,1024]{2,1,0:T(8,128)(2,1)} %bitcast.74), calls=%async_computation.1 | async-start | bytes 4194304 | tf_op jit(solution)/shard_map/all_to_all | solution.py:140
  105.3 21.2 %all-gather.8.cloned.1.call-done = bf16[1024,1024]{1,0:T(8,128)(2,1)} async-done(((bf16[128,1024]{1,0:T(8,128)(2,1)}), bf16[1024,1024]{1,0:T(8,128)(2,1)}) %all-gather.8.cloned.1.call-update) | async-done | bytes 2097168 | tf_op jit(solution)/shard_map/all_gather | solution.py:136
  126.5 5.9 %fusion.33 = bf16[1024,1024]{1,0:T(8,128)(2,1)} fusion(bf16[1024,1024]{1,0:T(8,128)(2,1)} %all-gather.8.cloned.1.call-done, bf16[1024,256]{1,0:T(8,128)(2,1)} %copy-done.9, bf16[1024,256]{1,0:T(8,128)(2,1)} %copy-done.10, bf16[1024,256]{1,0:T(8,128)(2,1)} %copy-done.11, bf16[1024,256]{1,0:T(8,128)(2,1)} %copy-done.12), kind=kOutput, calls=%fused_computation.64 | convolution fusion | flops 2155872256 | bytes 6291456 | tf_op jit(solution)/shard_map/dot_general | solution.py:137
  132.4 4.6 %all-to-all-start.2 = ((bf16[4,256,1024]{2,1,0:T(8,128)(2,1)}), bf16[4,256,1024]{2,1,0:T(8,128)(2,1)}, u32[]{:S(2)}, u32[]{:S(2)}) async-start(bf16[4,256,1024]{2,1,0:T(8,128)(2,1)} %bitcast.73), calls=%async_computation.2 | async-start | bytes 4194304 | tf_op jit(solution)/shard_map/all_to_all | solution.py:140
  137.9 5.1 %fusion.19 = f32[1024,768]{1,0:T(8,128)} fusion(bf16[1024,1024]{1,0:T(8,128)(2,1)S(1)} %bitcast.69, bf16[768,2048]{1,0:T(8,128)(2,1)} %bitcast.101), kind=kOutput, calls=%fused_computation.32 | convolution fusion | flops 1610612736 | bytes 6815744 | tf_op jit(solution)/shard_map/td,fd->tf/dot_general | solution.py:145
  143.0 3.5 %fusion.23 = f32[1024,768]{1,0:T(8,128)} fusion(bf16[1024,1024]{1,0:T(8,128)(2,1)S(1)} %bitcast.70, bf16[768,2048]{1,0:T(8,128)(2,1)S(1)} %bitcast.99), kind=kOutput, calls=%fused_computation.36 | convolution fusion | flops 1610612736 | bytes 6815744 | tf_op jit(solution)/shard_map/td,fd->tf/dot_general | solution.py:145
  146.5 16.0 %all-to-all-done.2 = bf16[4,256,1024]{2,1,0:T(8,128)(2,1)} async-done(((bf16[4,256,1024]{2,1,0:T(8,128)(2,1)}), bf16[4,256,1024]{2,1,0:T(8,128)(2,1)}, u32[]{:S(2)}, u32[]{:S(2)}) %all-to-all-start.2) | async-done | bytes 2097184 | tf_op jit(solution)/shard_map/all_to_all | solution.py:140
  162.5 4.0 %fusion.21 = f32[1024,768]{1,0:T(8,128)S(1)} fusion(bf16[1024,1024]{1,0:T(8,128)(2,1)} %bitcast.27, bf16[768,2048]{1,0:T(8,128)(2,1)} %bitcast.98), kind=kOutput, calls=%fused_computation.34 | convolution fusion | flops 1610612736 | bytes 6815744 | tf_op jit(solution)/shard_map/td,fd->tf/dot_general | solution.py:145
  167.3 4.1 %multiply_convert_fusion.1 = bf16[1024,768]{1,0:T(8,128)(2,1)S(1)} fusion(f32[1024,768]{1,0:T(8,128)S(1)} %copy-done.25, f32[1024,768]{1,0:T(8,128)S(1)} %copy-done.26, f32[1024,768]{1,0:T(8,128)S(1)} %fusion.21, bf16[1024,1024]{1,0:T(8,128)(2,1)} %bitcast.27, bf16[768,2048]{1,0:T(8,128)(2,1)S(1)} %bitcast.102), kind=kOutput, calls=%fused_computation.7 | convolution fusion | flops 1616904192 | bytes 14680064 | tf_op jit(solution)/shard_map/td,fd->tf/dot_general | solution.py:145
  171.4 1.8 fusion.6
  173.2 3.9 %fusion.12 = f32[1024,768]{1,0:T(8,128)S(1)} fusion(bf16[1024,1024]{1,0:T(8,128)(2,1)} %bitcast.27, bf16[768,2048]{1,0:T(8,128)(2,1)} %collective-permute-done.1), kind=kOutput, calls=%fused_computation.25 | convolution fusion | flops 1610612736 | bytes 6815744 | tf_op jit(solution)/shard_map/td,fd->tf/dot_general | solution.py:145
  177.1 3.2 %fusion.14 = f32[1024,768]{1,0:T(8,128)S(1)} fusion(bf16[1024,1024]{1,0:T(8,128)(2,1)S(1)} %bitcast.71, bf16[768,2048]{1,0:T(8,128)(2,1)} %collective-permute-done.1), kind=kOutput, calls=%fused_computation.27 | convolution fusion | flops 1610612736 | bytes 6815744 | tf_op jit(solution)/shard_map/td,fd->tf/dot_general | solution.py:145
  180.3 3.9 %fusion.9 = f32[1024,768]{1,0:T(8,128)S(1)} fusion(bf16[1024,1024]{1,0:T(8,128)(2,1)} %bitcast.27, bf16[768,2048]{1,0:T(8,128)(2,1)} %collective-permute-done.2), kind=kOutput, calls=%fused_computation.22 | convolution fusion | flops 1610612736 | bytes 6815744 | tf_op jit(solution)/shard_map/td,fd->tf/dot_general | solution.py:145
  184.2 4.0 %multiply_convert_fusion = bf16[1024,768]{1,0:T(8,128)(2,1)S(1)} fusion(f32[1024,768]{1,0:T(8,128)S(1)} %fusion.9, f32[1024,768]{1,0:T(8,128)S(1)} %fusion.14, f32[1024,768]{1,0:T(8,128)S(1)} %fusion.12, bf16[1024,1024]{1,0:T(8,128)(2,1)S(1)} %bitcast.72, bf16[768,2048]{1,0:T(8,128)(2,1)} %collective-permute-done.2), kind=kOutput, calls=%fused_computation.6 | convolution fusion | flops 1616904192 | bytes 14680064 | tf_op jit(solution)/shard_map/td,fd->tf/dot_general | solution.py:145
  188.2 5.1 %add_convert_fusion.1 = bf16[1024,1024]{1,0:T(8,128)(2,1)} fusion(f32[1024,1024]{1,0:T(8,128)S(1)} %fusion.6, bf16[1024,768]{1,0:T(8,128)(2,1)S(1)} %multiply_convert_fusion, bf16[768,2048]{1,0:T(8,128)(2,1)} %collective-permute-done.3), kind=kOutput, calls=%fused_computation.1 | convolution fusion | flops 1612709888 | bytes 9437184 | tf_op jit(solution)/shard_map/dot_general | solution.py:158
  193.3 4.6 %all-to-all-start.4 = ((bf16[4,256,1024]{2,1,0:T(8,128)(2,1)}), bf16[4,256,1024]{2,1,0:T(8,128)(2,1)}, u32[]{:S(2)}, u32[]{:S(2)}) async-start(bf16[4,256,1024]{2,1,0:T(8,128)(2,1)} %bitcast.32), calls=%async_computation.5 | async-start | bytes 4194304 | tf_op jit(solution)/shard_map/all_to_all | solution.py:160
  204.4 18.3 %all-to-all-done.4 = bf16[4,256,1024]{2,1,0:T(8,128)(2,1)} async-done(((bf16[4,256,1024]{2,1,0:T(8,128)(2,1)}), bf16[4,256,1024]{2,1,0:T(8,128)(2,1)}, u32[]{:S(2)}, u32[]{:S(2)}) %all-to-all-start.4) | async-done | bytes 2097184 | tf_op jit(solution)/shard_map/all_to_all | solution.py:160
  222.7 4.0 %fusion.31 = f32[1024,1024]{1,0:T(8,128)S(1)} fusion(bf16[1024,1024]{1,0:T(8,128)(2,1)} %bitcast.33, bf16[1024,256]{1,0:T(8,128)(2,1)S(1)} %copy-done.5, bf16[1024,256]{1,0:T(8,128)(2,1)S(1)} %copy-done.6, bf16[1024,256]{1,0:T(8,128)(2,1)S(1)} %copy-done.7, bf16[1024,256]{1,0:T(8,128)(2,1)S(1)} %copy-done.8), kind=kOutput, calls=%fused_computation.62 | convolution fusion | flops 2155872256 | bytes 8388608 | tf_op jit(solution)/shard_map/dot_general | solution.py:168
  226.6 2.1 add_convert_fusion
  228.8 3.8 %fusion.16 = f32[1024,1024]{1,0:T(8,128)S(1)} fusion(bf16[1024,768]{1,0:T(8,128)(2,1)} %copy-done.24, bf16[768,2048]{1,0:T(8,128)(2,1)} %bitcast.104), kind=kOutput, calls=%fused_computation.29 | convolution fusion | flops 1610612736 | bytes 7340032 | tf_op jit(solution)/shard_map/dot_general | solution.py:158
  232.6 3.3 %add_convert_fusion.3 = bf16[1024,1024]{1,0:T(8,128)(2,1)S(1)} fusion(f32[1024,1024]{1,0:T(8,128)S(1)} %fusion.16, bf16[1024,768]{1,0:T(8,128)(2,1)S(1)} %copy-done.28, bf16[768,2048]{1,0:T(8,128)(2,1)} %collective-permute-done.3), kind=kOutput, calls=%fused_computation.3 | convolution fusion | flops 1612709888 | bytes 9437184 | tf_op jit(solution)/shard_map/dot_general | solution.py:158
  235.9 27.3 %all_to_all.40 = bf16[4,256,1024]{2,1,0:T(8,128)(2,1)S(1)} all-to-all(bf16[4,256,1024]{2,1,0:T(8,128)(2,1)S(1)} %bitcast.76), channel_id=1, replica_groups=mesh['sp'=4,'tp'=8] {'sp'}, dimensions={0} | all-to-all | bytes 4194304 | tf_op jit(solution)/shard_map/all_to_all | solution.py:160
  263.2 2.3 fusion.32
  265.5 2.1 add_convert_fusion.2
  267.7 34.1 %reduce-scatter.3.cloned.1.call-done = bf16[128,1024]{1,0:T(8,128)(2,1)} async-done(((bf16[1024,1024]{1,0:T(8,128)(2,1)}), bf16[128,1024]{1,0:T(8,128)(2,1)}) %reduce-scatter.3.cloned.1.call-update) | async-done | bytes 262160 | tf_op jit(solution)/shard_map/reduce_scatter | solution.py:170
  301.8 1.9 add_convert_fusion.4
  (116 shorter events, 18.1 us)
Async XLA Ops:
  6.5 9.0 %copy-start.2 = (bf16[1024,256]{1,0:T(8,128)(2,1)S(1)}, bf16[1024,256]{1,0:T(8,128)(2,1)}, u32[]{:S(2)}) copy-start(bf16[1024,256]{1,0:T(8,128)(2,1)} %param.16) | copy-start | bytes 1572868
  6.5 9.0 %copy-start.3 = (bf16[1024,256]{1,0:T(8,128)(2,1)S(1)}, bf16[1024,256]{1,0:T(8,128)(2,1)}, u32[]{:S(2)}) copy-start(bf16[1024,256]{1,0:T(8,128)(2,1)} %param.17) | copy-start | bytes 1572868
  6.5 57.6 %all-gather.4.cloned.1.call-start = ((), (), s32[]{:S(2)}) async-start(), calls=%async_computation.7 | async-start | bytes 4718592 | tf_op jit(solution)/shard_map/all_gather | solution.py:115
  7.3 8.8 %copy-start.13 = (bf16[1024,128]{1,0:T(8,128)(2,1)S(1)}, bf16[1024,128]{1,0:T(8,128)(2,1)}, u32[]{:S(2)}) copy-start(bf16[1024,128]{1,0:T(8,128)(2,1)} %param.15) | copy-start | bytes 786436
  7.3 89.0 %all-gather.6.cloned.1.call-start = ((), (), s32[]{:S(2)}) async-start(), calls=%async_computation.8 | async-start | bytes 2359296 | tf_op jit(solution)/shard_map/all_gather | solution.py:136
  9.1 7.7 %collective-permute-start = (bf16[128,512]{1,0:T(8,128)(2,1)S(1)}, bf16[128,512]{1,0:T(8,128)(2,1)S(1)}, u32[]{:S(2)}, u32[]{:S(2)}) collective-permute-start(bf16[128,512]{1,0:T(8,128)(2,1)S(1)} %pad_maximum_fusion.6), channel_id=1, source_target_pairs={{0,8},{8,16},{16,24},{1,9},{9,17},{17,25},{2,10},{10,18},{18,26},{... | collective-permute-start | bytes 393224 | tf_op jit(solution)/shard_map/ppermute | solution.py:16
  18.2 46.0 %copy-start.4 = (bf16[128,2048]{1,0:T(8,128)(2,1)S(1)}, bf16[128,2048]{1,0:T(8,128)(2,1)}, u32[]{:S(2)}) copy-start(bf16[128,2048]{1,0:T(8,128)(2,1)} %param.20) | copy-start | bytes 1572868
  68.3 58.2 %all-gather.8.cloned.1.call-start = ((), (), s32[]{:S(2)}) async-start(), calls=%async_computation.9 | async-start | bytes 2359296 | tf_op jit(solution)/shard_map/all_gather | solution.py:136
  70.0 31.6 %copy-start.9 = (bf16[1024,256]{1,0:T(8,128)(2,1)}, bf16[1024,256]{1,0:T(8,128)(2,1)S(1)}, u32[]{:S(2)}) copy-start(bf16[1024,256]{1,0:T(8,128)(2,1)S(1)} %get-tuple-element.29) | copy-start | bytes 1572868
  70.0 31.6 %copy-start.10 = (bf16[1024,256]{1,0:T(8,128)(2,1)}, bf16[1024,256]{1,0:T(8,128)(2,1)S(1)}, u32[]{:S(2)}) copy-start(bf16[1024,256]{1,0:T(8,128)(2,1)S(1)} %get-tuple-element.30) | copy-start | bytes 1572868
  70.4 31.2 %copy-start.11 = (bf16[1024,256]{1,0:T(8,128)(2,1)}, bf16[1024,256]{1,0:T(8,128)(2,1)S(1)}, u32[]{:S(2)}) copy-start(bf16[1024,256]{1,0:T(8,128)(2,1)S(1)} %get-tuple-element.31) | copy-start | bytes 1572868
  70.4 31.2 %copy-start.12 = (bf16[1024,256]{1,0:T(8,128)(2,1)}, bf16[1024,256]{1,0:T(8,128)(2,1)S(1)}, u32[]{:S(2)}) copy-start(bf16[1024,256]{1,0:T(8,128)(2,1)S(1)} %get-tuple-element.32) | copy-start | bytes 1572868
  101.6 30.8 %all-to-all-start.1 = ((bf16[4,256,1024]{2,1,0:T(8,128)(2,1)}), bf16[4,256,1024]{2,1,0:T(8,128)(2,1)S(1)}, u32[]{:S(2)}, u32[]{:S(2)}) async-start(bf16[4,256,1024]{2,1,0:T(8,128)(2,1)} %bitcast.74), calls=%async_computation.1 | async-start | bytes 4194304 | tf_op jit(solution)/shard_map/all_to_all | solution.py:140
  132.4 30.1 %all-to-all-start.2 = ((bf16[4,256,1024]{2,1,0:T(8,128)(2,1)}), bf16[4,256,1024]{2,1,0:T(8,128)(2,1)}, u32[]{:S(2)}, u32[]{:S(2)}) async-start(bf16[4,256,1024]{2,1,0:T(8,128)(2,1)} %bitcast.73), calls=%async_computation.2 | async-start | bytes 4194304 | tf_op jit(solution)/shard_map/all_to_all | solution.py:140
  137.0 36.2 %collective-permute-start.1 = (bf16[768,2048]{1,0:T(8,128)(2,1)}, bf16[768,2048]{1,0:T(8,128)(2,1)}, u32[]{:S(2)}, u32[]{:S(2)}) collective-permute-start(bf16[768,2048]{1,0:T(8,128)(2,1)} %bitcast.97), channel_id=1, source_target_pairs={{0,1},{1,0},{2,3},{3,2},{4,5},{5,4},{6,7},{7,6},{8,9},{9,8},{10,11... | collective-permute-start | bytes 9437192 | tf_op jit(solution)/shard_map/ppermute | solution.py:20
  137.3 43.0 %collective-permute-start.2 = (bf16[768,2048]{1,0:T(8,128)(2,1)}, bf16[768,2048]{1,0:T(8,128)(2,1)}, u32[]{:S(2)}, u32[]{:S(2)}) collective-permute-start(bf16[768,2048]{1,0:T(8,128)(2,1)} %bitcast.100), channel_id=1, source_target_pairs={{0,1},{1,0},{2,3},{3,2},{4,5},{5,4},{6,7},{7,6},{8,9},{9,8},{10,11... | collective-permute-start | bytes 9437192 | tf_op jit(solution)/shard_map/ppermute | solution.py:20
  137.6 50.6 %collective-permute-start.3 = (bf16[768,2048]{1,0:T(8,128)(2,1)}, bf16[768,2048]{1,0:T(8,128)(2,1)}, u32[]{:S(2)}, u32[]{:S(2)}) collective-permute-start(bf16[768,2048]{1,0:T(8,128)(2,1)} %bitcast.103), channel_id=1, source_target_pairs={{0,1},{1,0},{2,3},{3,2},{4,5},{5,4},{6,7},{7,6},{8,9},{9,8},{10,11... | collective-permute-start | bytes 9437192 | tf_op jit(solution)/shard_map/ppermute | solution.py:20
  137.9 5.1 %copy-start.21 = (bf16[1,768,2048]{2,1,0:T(8,128)(2,1)S(1)}, bf16[1,768,2048]{2,1,0:T(8,128)(2,1)}, u32[]{:S(2)}) copy-start(bf16[1,768,2048]{2,1,0:T(8,128)(2,1)} %param.24) | copy-start | bytes 9437188
  162.5 4.0 %copy-start.22 = (bf16[1,768,2048]{2,1,0:T(8,128)(2,1)S(1)}, bf16[1,768,2048]{2,1,0:T(8,128)(2,1)}, u32[]{:S(2)}) copy-start(bf16[1,768,2048]{2,1,0:T(8,128)(2,1)} %param.25) | copy-start | bytes 9437188
  162.5 4.0 %copy-start.25 = (f32[1024,768]{1,0:T(8,128)S(1)}, f32[1024,768]{1,0:T(8,128)}, u32[]{:S(2)}) copy-start(f32[1024,768]{1,0:T(8,128)} %fusion.19) | copy-start | bytes 9437188
  162.5 4.9 %copy-start.26 = (f32[1024,768]{1,0:T(8,128)S(1)}, f32[1024,768]{1,0:T(8,128)}, u32[]{:S(2)}) copy-start(f32[1024,768]{1,0:T(8,128)} %fusion.23) | copy-start | bytes 9437188
  167.3 4.1 %copy-start.23 = (bf16[1,768,2048]{2,1,0:T(8,128)(2,1)S(1)}, bf16[1,768,2048]{2,1,0:T(8,128)(2,1)}, u32[]{:S(2)}) copy-start(bf16[1,768,2048]{2,1,0:T(8,128)(2,1)} %param.26) | copy-start | bytes 9437188
  188.2 5.1 %copy-start.27 = (bf16[1024,768]{1,0:T(8,128)(2,1)}, bf16[1024,768]{1,0:T(8,128)(2,1)S(1)}, u32[]{:S(2)}) copy-start(bf16[1024,768]{1,0:T(8,128)(2,1)S(1)} %multiply_convert_fusion) | copy-start | bytes 4718596
  193.3 7.9 %copy-start.16 = (bf16[64,2048]{1,0:T(8,128)(2,1)S(1)}, bf16[64,2048]{1,0:T(8,128)(2,1)}, u32[]{:S(2)}) copy-start(bf16[64,2048]{1,0:T(8,128)(2,1)} %param.28) | copy-start | bytes 786436
  193.3 29.3 %all-to-all-start.4 = ((bf16[4,256,1024]{2,1,0:T(8,128)(2,1)}), bf16[4,256,1024]{2,1,0:T(8,128)(2,1)}, u32[]{:S(2)}, u32[]{:S(2)}) async-start(bf16[4,256,1024]{2,1,0:T(8,128)(2,1)} %bitcast.32), calls=%async_computation.5 | async-start | bytes 4194304 | tf_op jit(solution)/shard_map/all_to_all | solution.py:160
  197.9 69.8 %reduce-scatter.5.cloned.1.call-start = ((), (), s32[]{:S(2)}) async-start(), calls=%async_computation.11 | async-start | bytes 2359296 | tf_op jit(solution)/shard_map/reduce_scatter | solution.py:170
  197.9 4.0 %copy-start.15 = (bf16[64,2048]{1,0:T(8,128)(2,1)S(1)}, bf16[64,2048]{1,0:T(8,128)(2,1)}, u32[]{:S(2)}) copy-start(bf16[64,2048]{1,0:T(8,128)(2,1)} %param.27) | copy-start | bytes 786436
  203.5 19.1 %copy-start.5 = (bf16[1024,256]{1,0:T(8,128)(2,1)S(1)}, bf16[1024,256]{1,0:T(8,128)(2,1)}, u32[]{:S(2)}) copy-start(bf16[1024,256]{1,0:T(8,128)(2,1)} %get-tuple-element.33) | copy-start | bytes 1572868
  203.6 19.1 %copy-start.6 = (bf16[1024,256]{1,0:T(8,128)(2,1)S(1)}, bf16[1024,256]{1,0:T(8,128)(2,1)}, u32[]{:S(2)}) copy-start(bf16[1024,256]{1,0:T(8,128)(2,1)} %get-tuple-element.34) | copy-start | bytes 1572868
  203.6 19.1 %copy-start.7 = (bf16[1024,256]{1,0:T(8,128)(2,1)S(1)}, bf16[1024,256]{1,0:T(8,128)(2,1)}, u32[]{:S(2)}) copy-start(bf16[1024,256]{1,0:T(8,128)(2,1)} %get-tuple-element.35) | copy-start | bytes 1572868
  203.6 19.1 %copy-start.8 = (bf16[1024,256]{1,0:T(8,128)(2,1)S(1)}, bf16[1024,256]{1,0:T(8,128)(2,1)}, u32[]{:S(2)}) copy-start(bf16[1024,256]{1,0:T(8,128)(2,1)} %get-tuple-element.36) | copy-start | bytes 1572868
  228.7 73.1 %reduce-scatter.3.cloned.1.call-start = ((), (), s32[]{:S(2)}) async-start(), calls=%async_computation.10 | async-start | bytes 2359296 | tf_op jit(solution)/shard_map/reduce_scatter | solution.py:170
  (9 other events, 22.5 us)
Sparse Core Ops, SparseCore 0:
  8.9 55.2 all-gather.3
  68.4 27.8 all-gather.5
  97.9 28.5 all-gather.7
  228.9 34.5 reduce-scatter.4
  267.7 34.0 reduce-scatter.2

commit v2 on v1

--- a/solution.py
+++ b/solution.py
@@ -30,21 +30,24 @@
     named = route_ids[:, :, None] == targets[None, None, :]
     named_f = jnp.sum(named.astype(jnp.float32), axis=1)
     weight = jnp.sum(jnp.where(named, route_weights[:, :, None], 0.0), axis=1)
+    named_t = jnp.sum((route_ids.T[None] == targets[:, None, None]).astype(jnp.float32), axis=1)
     rows = route_ids.shape[0]
-    before = jnp.arange(rows)[:, None] > jnp.arange(rows)[None, :]
-    rank = jnp.dot(
-        before.astype(jnp.bfloat16),
-        named_f.astype(jnp.bfloat16),
-        preferred_element_type=jnp.float32,
+    steps = jnp.arange(rows)
+    earlier = (steps[None, :] < steps[:, None]).astype(jnp.bfloat16)
+    rank = jnp.dot(earlier, named_f.astype(jnp.bfloat16), preferred_element_type=jnp.float32)
+    rank_t = jnp.einsum(
+        "sq,pq->sp", named_t.astype(jnp.bfloat16), earlier, preferred_element_type=jnp.float32
     )
     place = jnp.where(named_f > 0, rank - first_rank, -1.0)
+    place_t = jnp.where(named_t > 0, rank_t - first_rank, -1.0)
     slots = jnp.arange(half_cap, dtype=jnp.float32)
     picks, mixes = [], []
     for s in range(targets.shape[0]):
+        hit_t = place_t[s : s + 1, :] == slots[:, None]
+        picks.append(jnp.where(hit_t, 1.0, 0.0).astype(jnp.bfloat16))
         hit = place[:, s : s + 1] == slots[None, :]
-        picks.append(jnp.where(hit, 1.0, 0.0).astype(jnp.bfloat16))
         mixes.append(jnp.where(hit, weight[:, s : s + 1], 0.0).astype(jnp.bfloat16))
-    return jnp.concatenate(picks, axis=1), jnp.concatenate(mixes, axis=1)
+    return jnp.concatenate(picks, axis=0), jnp.concatenate(mixes, axis=1)
 
 
 def body(
@@ -110,6 +113,9 @@
     attended = jnp.einsum("nhqs,nsd->nqhd", weights, values_ext, preferred_element_type=jnp.float32)
     attended = attended.astype(jnp.bfloat16).reshape(seq_rows, local_heads * HD)
     head_rows = lax.all_to_all(attended, "tp", split_axis=0, concat_axis=1, tiled=True)
+    head_rows, other_gate, other_up, other_down = lax.optimization_barrier(
+        (head_rows, other_gate, other_up, other_down)
+    )
     projected = jnp.dot(
         head_rows,
         lax.all_gather(w_out, "tp", axis=0, tiled=True),
@@ -134,9 +140,7 @@
     for c in range(CHUNKS):
         cols = slice(c * step, (c + 1) * step)
         rows = lax.all_gather(normed[:, cols], "tp", axis=0, tiled=True)
-        outgoing = lax.dot_general(
-            pick, rows, (((0,), (0,)), ((), ())), preferred_element_type=jnp.bfloat16
-        )
+        outgoing = jnp.dot(pick, rows, preferred_element_type=jnp.float32).astype(jnp.bfloat16)
         arrived = lax.all_to_all(
             outgoing.reshape(sp_count, half_cap, step), "sp", split_axis=0, concat_axis=0, tiled=True
         ).reshape(sp_count * half_cap, step)
@@ -152,18 +156,19 @@
     shared_hidden = (jax.nn.silu(shared[0]) * shared[1]).astype(jnp.bfloat16)
     hidden = [(jax.nn.silu(g) * u).astype(jnp.bfloat16) for g, u in sums]
     pieces = []
+    outs = []
     for c in range(CHUNKS):
         cols = slice(c * step, (c + 1) * step)
         expert_out = sum(
             jnp.dot(h, w[:, cols], preferred_element_type=jnp.float32) for h, w in zip(hidden, downs)
         ).astype(jnp.bfloat16)
-        held = lax.all_to_all(
-            expert_out.reshape(sp_count, half_cap, step),
-            "sp",
-            split_axis=0,
-            concat_axis=0,
-            tiled=True,
-        ).reshape(sp_count * half_cap, step)
+        outs.append(expert_out.reshape(sp_count, half_cap, step))
+    for c in range(CHUNKS):
+        cols = slice(c * step, (c + 1) * step)
+        held = lax.all_to_all(outs[c], "sp", split_axis=0, concat_axis=0, tiled=True)
+        if c + 1 < CHUNKS:
+            held, outs[c + 1] = lax.optimization_barrier((held, outs[c + 1]))
+        held = held.reshape(sp_count * half_cap, step)
         part = jnp.dot(shared_hidden, shared_down[:, cols], preferred_element_type=jnp.float32)
         part = part + jnp.dot(mix, held, preferred_element_type=jnp.float32)
         pieces.append(

time: 311 us -> 310 us (level)
  waiting for transfers between devices: 140 us -> 136 us
    reduce_scatter x2, waiting for transfers between devices: 34.2 us -> 39.4 us  [body(): lax.psum_scatter(part.astype(jnp.bfloat16), 'tp', scatter_dimension=0, ti...]
    all_to_all x2, waiting for transfers between devices: 16 us -> 12 us  [body(): lax.all_to_all(outgoing.reshape(sp_count, half_cap, step), 'sp', split_ax...]
    all_to_all x1, waiting for transfers between devices: 18.3 us -> 14.3 us  [body(): lax.all_to_all(outs[c], 'sp', split_axis=0, concat_axis=0, tiled=True)]
    dot_general x3 -> x4, matrix products: 11.7 us -> 12.1 us  [the longest x2 11.2 us: body(): jnp.dot(pick, rows, preferred_element_type=jnp.float32).astype(jnp.bfloat16)]
  transfers between devices with their start and end apart: 12 -> 12, of which waited for: 6 -> 8; matrix products, arithmetic and copies ran while one was open for 22% -> 16% of each run, Pallas kernels for 0% -> 0%
where the time goes in v2:
time: 310 us; the launch traced here: 309 us
  waiting for transfers between devices  136 us (44%)
  matrix products  77.5 us (25%)
  blocking collectives  49.5 us (16%)
  starting transfers between devices  18.4 us (6%)
  between operations  13.8 us (4%)
  local copies, waits for them, and re-layouts  7.29 us (2%)
  other arithmetic  6.95 us (2%)
    all_gather x2, waiting for transfers between devices, body(): rows = lax.all_gather(normed[:, cols], 'tp', axis=0, tiled=True)  45.2 us
    reduce_scatter x2, waiting for transfers between devices, body(): lax.psum_scatter(part.astype(jnp.bfloat16), 'tp', scatter_dimension=0, ti...  39.4 us
    dot_general x8, matrix products, body(): jnp.einsum('td,fd->tf', arrived, w[:, cols], preferred_element_type=jnp.f...  30.9 us
    all_to_all x1, blocking collectives, body(): lax.all_to_all(outs[c], 'sp', split_axis=0, concat_axis=0, tiled=True)  27.5 us
    all_gather x1, waiting for transfers between devices, body(): lax.all_gather(w_out, 'tp', axis=0, tiled=True)  22.7 us
    all_to_all x1, blocking collectives, body(): lax.all_to_all(attended, 'tp', split_axis=0, concat_axis=1, tiled=True)  22 us
    all_to_all x1, waiting for transfers between devices, body(): lax.all_to_all(outs[c], 'sp', split_axis=0, concat_axis=0, tiled=True)  14.3 us
    dot_general x4, matrix products, body(): jnp.dot(h, w[:, cols], preferred_element_type=jnp.float32)  13.7 us
  transfers between devices with their start and end apart: 12, of which 8 were waited for; matrix products, arithmetic and copies ran while one was open for 16% of the time, Pallas kernels for 0%

profile of v2, /device:TPU:0, one launch (start us, length us, event | category | flops | bytes accessed | tf_op | source)
XLA Modules:
  0.0 308.9 jit_solution(18365934539425625219)
XLA Ops:
  10.1 4.5 %collective-permute-start = (bf16[128,512]{1,0:T(8,128)(2,1)S(1)}, bf16[128,512]{1,0:T(8,128)(2,1)S(1)}, u32[]{:S(2)}, u32[]{:S(2)}) collective-permute-start(bf16[128,512]{1,0:T(8,128)(2,1)S(1)} %pad_maximum_fusion.6), channel_id=1, source_target_pairs={{0,8},{8,16},{16,24},{1,9},{9,17},{17,25},{2,10},{10,18},{18,26},{... | collective-permute-start | bytes 393224 | tf_op jit(solution)/shard_map/ppermute | solution.py:16
  19.6 22.0 %all_to_all.39 = bf16[8,128,128]{1,2,0:T(8,128)(2,1)S(1)} all-to-all(bf16[8,128,128]{1,2,0:T(8,128)(2,1)S(1)} %bitcast.88), channel_id=1, replica_groups=mesh['sp'=4,'tp'=8] {'tp'}, dimensions={0} | all-to-all | bytes 524288 | tf_op jit(solution)/shard_map/all_to_all | solution.py:115
  41.6 22.7 %all-gather.4.cloned.1.call-done = bf16[1024,2048]{1,0:T(8,128)(2,1)} async-done(((bf16[128,2048]{1,0:T(8,128)(2,1)}), bf16[1024,2048]{1,0:T(8,128)(2,1)}) %all-gather.4.cloned.1.call-update) | async-done | bytes 4194320 | tf_op jit(solution)/shard_map/all_gather | solution.py:121
  64.2 3.0 multiply_reduce_fusion
  70.2 26.1 %all-gather.8.cloned.1.call-done = bf16[1024,1024]{1,0:T(8,128)(2,1)} async-done(((bf16[128,1024]{1,0:T(8,128)(2,1)}), bf16[1024,1024]{1,0:T(8,128)(2,1)}) %all-gather.8.cloned.1.call-update) | async-done | bytes 2097168 | tf_op jit(solution)/shard_map/all_gather | solution.py:142
  96.3 5.2 %convolution_convert_fusion = bf16[1024,1024]{1,0:T(8,128)(2,1)} fusion(bf16[1024,1024]{1,0:T(8,128)(2,1)} %all-gather.8.cloned.1.call-done, bf16[256,1024]{1,0:T(8,128)(2,1)S(1)} %get-tuple-element.45, bf16[256,1024]{1,0:T(8,128)(2,1)S(1)} %get-tuple-element.46, bf16[256,1024]{1,0:T(8,128)(2,1)S(1)} %get-tuple-element.47, ...), kind=kOutput, calls=%fused_computation.19 | convolution fusion | flops 2156920832 | bytes 6291456 | tf_op jit(solution)/shard_map/dot_general | solution.py:143
  101.6 3.7 %all-to-all-start.2 = ((bf16[4,256,1024]{2,1,0:T(8,128)(2,1)}), bf16[4,256,1024]{2,1,0:T(8,128)(2,1)S(1)}, u32[]{:S(2)}, u32[]{:S(2)}) async-start(bf16[4,256,1024]{2,1,0:T(8,128)(2,1)} %bitcast.78), calls=%async_computation.2 | async-start | bytes 4194304 | tf_op jit(solution)/shard_map/all_to_all | solution.py:144
  107.5 19.2 %all-gather.6.cloned.1.call-done = bf16[1024,1024]{1,0:T(8,128)(2,1)} async-done(((bf16[128,1024]{1,0:T(8,128)(2,1)}), bf16[1024,1024]{1,0:T(8,128)(2,1)}) %all-gather.6.cloned.1.call-update) | async-done | bytes 2097168 | tf_op jit(solution)/shard_map/all_gather | solution.py:142
  126.7 5.9 %convolution_convert_fusion.1 = bf16[1024,1024]{1,0:T(8,128)(2,1)} fusion(bf16[1024,1024]{1,0:T(8,128)(2,1)} %all-gather.6.cloned.1.call-done, bf16[256,1024]{1,0:T(8,128)(2,1)} %copy-done.13, bf16[256,1024]{1,0:T(8,128)(2,1)} %copy-done.14, bf16[256,1024]{1,0:T(8,128)(2,1)} %copy-done.15, bf16[256,1024]{1,0:T(8,128)(2,1)} %copy-done.16), kind=kOutput, calls=%fused_computation.20 | convolution fusion | flops 2156920832 | bytes 6291456 | tf_op jit(solution)/shard_map/dot_general | solution.py:143
  134.0 4.6 %all-to-all-start.1 = ((bf16[4,256,1024]{2,1,0:T(8,128)(2,1)}), bf16[4,256,1024]{2,1,0:T(8,128)(2,1)}, u32[]{:S(2)}, u32[]{:S(2)}) async-start(bf16[4,256,1024]{2,1,0:T(8,128)(2,1)} %bitcast.79), calls=%async_computation.1 | async-start | bytes 4194304 | tf_op jit(solution)/shard_map/all_to_all | solution.py:144
  142.5 4.8 %fusion.13 = f32[1024,768]{1,0:T(8,128)} fusion(bf16[1024,1024]{1,0:T(8,128)(2,1)S(1)} %bitcast.74, bf16[768,2048]{1,0:T(8,128)(2,1)} %bitcast.105), kind=kOutput, calls=%fused_computation.28 | convolution fusion | flops 1610612736 | bytes 6815744 | tf_op jit(solution)/shard_map/td,fd->tf/dot_general | solution.py:149
  147.3 4.9 %fusion.22 = f32[1024,768]{1,0:T(8,128)} fusion(bf16[1024,1024]{1,0:T(8,128)(2,1)S(1)} %bitcast.75, bf16[768,2048]{1,0:T(8,128)(2,1)} %collective-permute-done.1), kind=kOutput, calls=%fused_computation.37 | convolution fusion | flops 1610612736 | bytes 6815744 | tf_op jit(solution)/shard_map/td,fd->tf/dot_general | solution.py:149
  152.2 12.0 %all-to-all-done.1 = bf16[4,256,1024]{2,1,0:T(8,128)(2,1)} async-done(((bf16[4,256,1024]{2,1,0:T(8,128)(2,1)}), bf16[4,256,1024]{2,1,0:T(8,128)(2,1)}, u32[]{:S(2)}, u32[]{:S(2)}) %all-to-all-start.1) | async-done | bytes 2097184 | tf_op jit(solution)/shard_map/all_to_all | solution.py:144
  164.2 4.0 %fusion.24 = f32[1024,768]{1,0:T(8,128)S(1)} fusion(bf16[1024,1024]{1,0:T(8,128)(2,1)} %bitcast.32, bf16[768,2048]{1,0:T(8,128)(2,1)} %collective-permute-done.1), kind=kOutput, calls=%fused_computation.39 | convolution fusion | flops 1610612736 | bytes 6815744 | tf_op jit(solution)/shard_map/td,fd->tf/dot_general | solution.py:149
  168.2 3.6 %fusion.11 = f32[1024,768]{1,0:T(8,128)S(1)} fusion(bf16[1024,1024]{1,0:T(8,128)(2,1)} %bitcast.32, bf16[768,2048]{1,0:T(8,128)(2,1)S(1)} %bitcast.108), kind=kOutput, calls=%fused_computation.26 | convolution fusion | flops 1610612736 | bytes 6815744 | tf_op jit(solution)/shard_map/td,fd->tf/dot_general | solution.py:149
  171.8 3.6 %fusion.15 = f32[1024,768]{1,0:T(8,128)S(1)} fusion(bf16[1024,1024]{1,0:T(8,128)(2,1)} %bitcast.32, bf16[768,2048]{1,0:T(8,128)(2,1)S(1)} %bitcast.106), kind=kOutput, calls=%fused_computation.30 | convolution fusion | flops 1610612736 | bytes 6815744 | tf_op jit(solution)/shard_map/td,fd->tf/dot_general | solution.py:149
  175.4 3.4 %fusion.19 = f32[1024,768]{1,0:T(8,128)S(1)} fusion(bf16[1024,1024]{1,0:T(8,128)(2,1)S(1)} %bitcast.76, bf16[768,2048]{1,0:T(8,128)(2,1)} %collective-permute-done.2), kind=kOutput, calls=%fused_computation.34 | convolution fusion | flops 1610612736 | bytes 6815744 | tf_op jit(solution)/shard_map/td,fd->tf/dot_general | solution.py:149
  178.8 2.3 multiply_convert_fusion.1
  181.1 2.0 fusion.8
  183.6 4.3 %multiply_convert_fusion = bf16[1024,768]{1,0:T(8,128)(2,1)S(1)} fusion(f32[1024,768]{1,0:T(8,128)S(1)} %fusion.19, f32[1024,768]{1,0:T(8,128)S(1)} %fusion.24, f32[1024,768]{1,0:T(8,128)S(1)} %copy-done.30, bf16[1024,1024]{1,0:T(8,128)(2,1)} %bitcast.32, bf16[768,2048]{1,0:T(8,128)(2,1)} %collective-permute-done.2), kind=kOutput, calls=%fused_computation.7 | convolution fusion | flops 1616904192 | bytes 14680064 | tf_op jit(solution)/shard_map/td,fd->tf/dot_general | solution.py:149
  187.9 5.1 %add_convert_fusion.3 = bf16[1024,1024]{1,0:T(8,128)(2,1)} fusion(f32[1024,1024]{1,0:T(8,128)S(1)} %fusion.8, bf16[1024,768]{1,0:T(8,128)(2,1)S(1)} %multiply_convert_fusion, bf16[768,2048]{1,0:T(8,128)(2,1)} %collective-permute-done.3), kind=kOutput, calls=%fused_computation.3 | convolution fusion | flops 1612709888 | bytes 9437184 | tf_op jit(solution)/shard_map/dot_general | solution.py:163
  193.1 4.5 %all-to-all-start.3 = ((bf16[4,256,1024]{2,1,0:T(8,128)(2,1)}), bf16[4,256,1024]{2,1,0:T(8,128)(2,1)}, u32[]{:S(2)}, u32[]{:S(2)}) async-start(bf16[4,256,1024]{2,1,0:T(8,128)(2,1)} %bitcast.81), calls=%async_computation.3 | async-start | bytes 4194304 | tf_op jit(solution)/shard_map/all_to_all | solution.py:168
  201.4 3.3 %fusion.6 = f32[1024,1024]{1,0:T(8,128)S(1)} fusion(bf16[1024,768]{1,0:T(8,128)(2,1)} %copy-done.29, bf16[768,2048]{1,0:T(8,128)(2,1)S(1)} %bitcast.112), kind=kOutput, calls=%fused_computation.21 | convolution fusion | flops 1610612736 | bytes 7340032 | tf_op jit(solution)/shard_map/dot_general | solution.py:163
  204.7 3.2 %add_convert_fusion.2 = bf16[1024,1024]{1,0:T(8,128)(2,1)S(1)} fusion(f32[1024,1024]{1,0:T(8,128)S(1)} %fusion.6, bf16[1024,768]{1,0:T(8,128)(2,1)S(1)} %copy-done.33, bf16[768,2048]{1,0:T(8,128)(2,1)} %collective-permute-done.3), kind=kOutput, calls=%fused_computation.2 | convolution fusion | flops 1612709888 | bytes 9437184 | tf_op jit(solution)/shard_map/dot_general | solution.py:163
  208.0 14.3 %all-to-all-done.3 = bf16[4,256,1024]{2,1,0:T(8,128)(2,1)} async-done(((bf16[4,256,1024]{2,1,0:T(8,128)(2,1)}), bf16[4,256,1024]{2,1,0:T(8,128)(2,1)}, u32[]{:S(2)}, u32[]{:S(2)}) %all-to-all-start.3) | async-done | bytes 2097184 | tf_op jit(solution)/shard_map/all_to_all | solution.py:168
  222.3 4.6 %fusion.35 = f32[1024,1024]{1,0:T(8,128)S(1)} fusion(bf16[1024,1024]{1,0:T(8,128)(2,1)} %bitcast.37, bf16[1024,256]{1,0:T(8,128)(2,1)} %get-tuple-element.49, bf16[1024,256]{1,0:T(8,128)(2,1)} %get-tuple-element.50, bf16[1024,256]{1,0:T(8,128)(2,1)} %get-tuple-element.51, bf16[1024,256]{1,0:T(8,128)(2,1)} %get-tuple-element.52), kind=kOutput, calls=%fused_computation.72 | convolution fusion | flops 2155872256 | bytes 8388608 | tf_op jit(solution)/shard_map/dot_general | solution.py:173
  226.9 2.1 add_convert_fusion.1
  229.1 27.5 %all_to_all.40 = bf16[4,256,1024]{2,1,0:T(8,128)(2,1)S(1)} all-to-all(bf16[4,256,1024]{2,1,0:T(8,128)(2,1)S(1)} %bitcast.80), channel_id=1, replica_groups=mesh['sp'=4,'tp'=8] {'sp'}, dimensions={0} | all-to-all | bytes 4194304 | tf_op jit(solution)/shard_map/all_to_all | solution.py:168
  256.6 2.3 fusion.34
  258.9 2.1 add_convert_fusion
  261.0 2.5 reduce-scatter.3.cloned.1.call-done
  263.6 36.9 %reduce-scatter.5.cloned.1.call-done = bf16[128,1024]{1,0:T(8,128)(2,1)} async-done(((bf16[1024,1024]{1,0:T(8,128)(2,1)}), bf16[128,1024]{1,0:T(8,128)(2,1)}) %reduce-scatter.5.cloned.1.call-update) | async-done | bytes 262160 | tf_op jit(solution)/shard_map/reduce_scatter | solution.py:175
  (129 shorter events, 25.1 us)
Async XLA Ops:
  6.5 9.6 %copy-start.6 = (bf16[1024,256]{1,0:T(8,128)(2,1)S(1)}, bf16[1024,256]{1,0:T(8,128)(2,1)}, u32[]{:S(2)}) copy-start(bf16[1024,256]{1,0:T(8,128)(2,1)} %param.16) | copy-start | bytes 1572868
  6.5 9.6 %copy-start.7 = (bf16[1024,256]{1,0:T(8,128)(2,1)S(1)}, bf16[1024,256]{1,0:T(8,128)(2,1)}, u32[]{:S(2)}) copy-start(bf16[1024,256]{1,0:T(8,128)(2,1)} %param.17) | copy-start | bytes 1572868
  6.5 57.7 %all-gather.4.cloned.1.call-start = ((), (), s32[]{:S(2)}) async-start(), calls=%async_computation.7 | async-start | bytes 4718592 | tf_op jit(solution)/shard_map/all_gather | solution.py:121
  7.3 9.4 %copy-start.17 = (bf16[1024,128]{1,0:T(8,128)(2,1)S(1)}, bf16[1024,128]{1,0:T(8,128)(2,1)}, u32[]{:S(2)}) copy-start(bf16[1024,128]{1,0:T(8,128)(2,1)} %param.15) | copy-start | bytes 786436
  7.3 89.0 %all-gather.8.cloned.1.call-start = ((), (), s32[]{:S(2)}) async-start(), calls=%async_computation.9 | async-start | bytes 2359296 | tf_op jit(solution)/shard_map/all_gather | solution.py:142
  7.3 34.2 %collective-permute-start.1 = (bf16[768,2048]{1,0:T(8,128)(2,1)}, bf16[768,2048]{1,0:T(8,128)(2,1)}, u32[]{:S(2)}, u32[]{:S(2)}) collective-permute-start(bf16[768,2048]{1,0:T(8,128)(2,1)} %bitcast.104), channel_id=1, source_target_pairs={{0,1},{1,0},{2,3},{3,2},{4,5},{5,4},{6,7},{7,6},{8,9},{9,8},{10,11... | collective-permute-start | bytes 9437192 | tf_op jit(solution)/shard_map/ppermute | solution.py:20
  7.9 33.7 %collective-permute-start.2 = (bf16[768,2048]{1,0:T(8,128)(2,1)}, bf16[768,2048]{1,0:T(8,128)(2,1)}, u32[]{:S(2)}, u32[]{:S(2)}) collective-permute-start(bf16[768,2048]{1,0:T(8,128)(2,1)} %bitcast.107), channel_id=1, source_target_pairs={{0,1},{1,0},{2,3},{3,2},{4,5},{5,4},{6,7},{7,6},{8,9},{9,8},{10,11... | collective-permute-start | bytes 9437192 | tf_op jit(solution)/shard_map/ppermute | solution.py:20
  8.0 33.6 %collective-permute-start.3 = (bf16[768,2048]{1,0:T(8,128)(2,1)}, bf16[768,2048]{1,0:T(8,128)(2,1)}, u32[]{:S(2)}, u32[]{:S(2)}) collective-permute-start(bf16[768,2048]{1,0:T(8,128)(2,1)} %bitcast.110), channel_id=1, source_target_pairs={{0,1},{1,0},{2,3},{3,2},{4,5},{5,4},{6,7},{7,6},{8,9},{9,8},{10,11... | collective-permute-start | bytes 9437192 | tf_op jit(solution)/shard_map/ppermute | solution.py:20
  10.1 7.8 %collective-permute-start = (bf16[128,512]{1,0:T(8,128)(2,1)S(1)}, bf16[128,512]{1,0:T(8,128)(2,1)S(1)}, u32[]{:S(2)}, u32[]{:S(2)}) collective-permute-start(bf16[128,512]{1,0:T(8,128)(2,1)S(1)} %pad_maximum_fusion.6), channel_id=1, source_target_pairs={{0,8},{8,16},{16,24},{1,9},{9,17},{17,25},{2,10},{10,18},{18,26},{... | collective-permute-start | bytes 393224 | tf_op jit(solution)/shard_map/ppermute | solution.py:16
  19.2 45.0 %copy-start.8 = (bf16[128,2048]{1,0:T(8,128)(2,1)S(1)}, bf16[128,2048]{1,0:T(8,128)(2,1)}, u32[]{:S(2)}) copy-start(bf16[128,2048]{1,0:T(8,128)(2,1)} %param.20) | copy-start | bytes 1572868
  41.6 25.7 %copy-start.23 = (f32[2048]{0:T(1024)S(1)}, f32[2048]{0:T(1024)}, u32[]{:S(2)}) copy-start(f32[2048]{0:T(1024)} %param.21) | copy-start | bytes 24580
  68.3 58.3 %all-gather.6.cloned.1.call-start = ((), (), s32[]{:S(2)}) async-start(), calls=%async_computation.8 | async-start | bytes 2359296 | tf_op jit(solution)/shard_map/all_gather | solution.py:142
  70.0 31.6 %copy-start.13 = (bf16[256,1024]{1,0:T(8,128)(2,1)}, bf16[256,1024]{1,0:T(8,128)(2,1)S(1)}, u32[]{:S(2)}) copy-start(bf16[256,1024]{1,0:T(8,128)(2,1)S(1)} %get-tuple-element.45) | copy-start | bytes 1572868
  70.0 31.6 %copy-start.14 = (bf16[256,1024]{1,0:T(8,128)(2,1)}, bf16[256,1024]{1,0:T(8,128)(2,1)S(1)}, u32[]{:S(2)}) copy-start(bf16[256,1024]{1,0:T(8,128)(2,1)S(1)} %get-tuple-element.46) | copy-start | bytes 1572868
  70.2 31.3 %copy-start.15 = (bf16[256,1024]{1,0:T(8,128)(2,1)}, bf16[256,1024]{1,0:T(8,128)(2,1)S(1)}, u32[]{:S(2)}) copy-start(bf16[256,1024]{1,0:T(8,128)(2,1)S(1)} %get-tuple-element.47) | copy-start | bytes 1572868
  70.2 31.3 %copy-start.16 = (bf16[256,1024]{1,0:T(8,128)(2,1)}, bf16[256,1024]{1,0:T(8,128)(2,1)S(1)}, u32[]{:S(2)}) copy-start(bf16[256,1024]{1,0:T(8,128)(2,1)S(1)} %get-tuple-element.48) | copy-start | bytes 1572868
  101.6 3.7 %copy-start.22 = (f32[1024,4]{0,1:T(4,128)S(1)}, f32[1024,4]{0,1:T(4,128)}, u32[]{:S(2)}) copy-start(f32[1024,4]{0,1:T(4,128)} %param.23) | copy-start | bytes 49156
  101.6 31.0 %all-to-all-start.2 = ((bf16[4,256,1024]{2,1,0:T(8,128)(2,1)}), bf16[4,256,1024]{2,1,0:T(8,128)(2,1)S(1)}, u32[]{:S(2)}, u32[]{:S(2)}) async-start(bf16[4,256,1024]{2,1,0:T(8,128)(2,1)} %bitcast.78), calls=%async_computation.2 | async-start | bytes 4194304 | tf_op jit(solution)/shard_map/all_to_all | solution.py:144
  134.0 6.2 %copy-start = (bf16[1024,1024]{1,0:T(8,128)(2,1)S(1)}, bf16[1024,1024]{1,0:T(8,128)(2,1)}, u32[]{:S(2)}) copy-start(bf16[1024,1024]{1,0:T(8,128)(2,1)} %all-gather.6.cloned.1.call-done) | copy-start | bytes 6291460
  134.0 6.2 %copy-start.19 = (bf16[64,2048]{1,0:T(8,128)(2,1)S(1)}, bf16[64,2048]{1,0:T(8,128)(2,1)}, u32[]{:S(2)}) copy-start(bf16[64,2048]{1,0:T(8,128)(2,1)} %param.27) | copy-start | bytes 786436
  134.0 30.2 %all-to-all-start.1 = ((bf16[4,256,1024]{2,1,0:T(8,128)(2,1)}), bf16[4,256,1024]{2,1,0:T(8,128)(2,1)}, u32[]{:S(2)}, u32[]{:S(2)}) async-start(bf16[4,256,1024]{2,1,0:T(8,128)(2,1)} %bitcast.79), calls=%async_computation.1 | async-start | bytes 4194304 | tf_op jit(solution)/shard_map/all_to_all | solution.py:144
  164.2 4.0 %copy-start.26 = (bf16[1,768,2048]{2,1,0:T(8,128)(2,1)S(1)}, bf16[1,768,2048]{2,1,0:T(8,128)(2,1)}, u32[]{:S(2)}) copy-start(bf16[1,768,2048]{2,1,0:T(8,128)(2,1)} %param.25) | copy-start | bytes 9437188
  168.2 3.6 %copy-start.25 = (bf16[1,768,2048]{2,1,0:T(8,128)(2,1)S(1)}, bf16[1,768,2048]{2,1,0:T(8,128)(2,1)}, u32[]{:S(2)}) copy-start(bf16[1,768,2048]{2,1,0:T(8,128)(2,1)} %param.24) | copy-start | bytes 9437188
  187.9 5.1 %copy-start.32 = (bf16[1024,768]{1,0:T(8,128)(2,1)}, bf16[1024,768]{1,0:T(8,128)(2,1)S(1)}, u32[]{:S(2)}) copy-start(bf16[1024,768]{1,0:T(8,128)(2,1)S(1)} %multiply_convert_fusion) | copy-start | bytes 4718596
  193.1 29.2 %all-to-all-start.3 = ((bf16[4,256,1024]{2,1,0:T(8,128)(2,1)}), bf16[4,256,1024]{2,1,0:T(8,128)(2,1)}, u32[]{:S(2)}, u32[]{:S(2)}) async-start(bf16[4,256,1024]{2,1,0:T(8,128)(2,1)} %bitcast.81), calls=%async_computation.3 | async-start | bytes 4194304 | tf_op jit(solution)/shard_map/all_to_all | solution.py:168
  197.5 66.0 %reduce-scatter.3.cloned.1.call-start = ((), (), s32[]{:S(2)}) async-start(), calls=%async_computation.10 | async-start | bytes 2359296 | tf_op jit(solution)/shard_map/reduce_scatter | solution.py:175
  222.3 4.6 %copy-start.18 = (bf16[64,2048]{1,0:T(8,128)(2,1)S(1)}, bf16[64,2048]{1,0:T(8,128)(2,1)}, u32[]{:S(2)}) copy-start(bf16[64,2048]{1,0:T(8,128)(2,1)} %param.29) | copy-start | bytes 786436
  229.0 71.4 %reduce-scatter.5.cloned.1.call-start = ((), (), s32[]{:S(2)}) async-start(), calls=%async_computation.11 | async-start | bytes 2359296 | tf_op jit(solution)/shard_map/reduce_scatter | solution.py:175
  229.1 27.5 %copy-start.9 = (bf16[1024,256]{1,0:T(8,128)(2,1)S(1)}, bf16[1024,256]{1,0:T(8,128)(2,1)}, u32[]{:S(2)}) copy-start(bf16[1024,256]{1,0:T(8,128)(2,1)} %get-tuple-element.49) | copy-start | bytes 1572868
  229.1 27.5 %copy-start.10 = (bf16[1024,256]{1,0:T(8,128)(2,1)S(1)}, bf16[1024,256]{1,0:T(8,128)(2,1)}, u32[]{:S(2)}) copy-start(bf16[1024,256]{1,0:T(8,128)(2,1)} %get-tuple-element.50) | copy-start | bytes 1572868
  229.1 27.5 %copy-start.11 = (bf16[1024,256]{1,0:T(8,128)(2,1)S(1)}, bf16[1024,256]{1,0:T(8,128)(2,1)}, u32[]{:S(2)}) copy-start(bf16[1024,256]{1,0:T(8,128)(2,1)} %get-tuple-element.51) | copy-start | bytes 1572868
  229.1 27.5 %copy-start.12 = (bf16[1024,256]{1,0:T(8,128)(2,1)S(1)}, bf16[1024,256]{1,0:T(8,128)(2,1)}, u32[]{:S(2)}) copy-start(bf16[1024,256]{1,0:T(8,128)(2,1)} %get-tuple-element.52) | copy-start | bytes 1572868
  (14 other events, 32.4 us)
Sparse Core Ops, SparseCore 0:
  8.9 55.2 all-gather.3
  68.4 27.8 all-gather.7
  97.9 28.6 all-gather.5
  229.1 34.3 reduce-scatter.2
  265.7 34.6 reduce-scatter.4
